TPU v7x, 32 devices: a whole 2x2x4 slice. The times are simulated.
32 devices in a mesh: grp: 2 (over y), ep: 16 (over z, x, core), tp: 1.
Axes of the slice: x: 2, y: 2, z: 4, core: 2. Of those that a mesh axis runs over, the one named last changes fastest.
Arguments:
- tokens: bfloat16 [3072, 2048], P(('grp', 'ep')), parts along dimension 0, may hold values from -6 to 6
- prior_state: float32 [2, 3072, 4096], P(None, ('grp', 'ep'), 'tp'), parts along dimension 1, may hold values from -6 to 6
- mix_gain: float32 [2048], replicated, may hold values from 0.1 to 1.9
- in_weight: bfloat16 [2048, 1024], P(None, 'tp'), may hold values from -0.125 to 0.125
- decay_rate: float32 [64, 64], P('tp'), may hold values from 0.2 to 20
- frequency: float32 [64, 64], P('tp'), may hold values from 0 to 12
- log_step: float32 [64], P('tp'), may hold values from -4.6 to 0
- input_map: float32 [2, 64, 64, 16], P(None, 'tp'), may hold values from -6 to 6
- output_map: float32 [2, 64, 16, 64], P(None, 'tp'), may hold values from -0.5 to 0.5
- skip_gain: float32 [1024], P('tp'), may hold values from -4 to 4
- out_weight: bfloat16 [1024, 2048], P('tp'), may hold values from -0.1875 to 0.1875
- channel_gain: float32 [2048], replicated, may hold values from 0.1 to 1.9
- expert_gate: bfloat16 [16, 2048, 512], P('ep', None, 'tp'), may hold values from -0.125 to 0.125
- expert_up: bfloat16 [16, 2048, 512], P('ep', None, 'tp'), may hold values from -0.125 to 0.125
- expert_down: bfloat16 [16, 512, 2048], P('ep', 'tp'), may hold values from -0.25 to 0.25
- shared_gate: bfloat16 [2048, 512], P(None, 'tp'), may hold values from -0.125 to 0.125
- shared_up: bfloat16 [2048, 512], P(None, 'tp'), may hold values from -0.125 to 0.125
- shared_down: bfloat16 [512, 2048], P('tp'), may hold values from -0.25 to 0.25
- routes: int32 [3072, 6], P(('grp', 'ep')), parts along dimension 0, may hold values from 0 to 15, all different within a row; in each aligned block of 96 rows (0 to 95, 96 to 191, ...) at most 54 rows name the same one
- route_weights: float32 [3072, 6], P(('grp', 'ep')), parts along dimension 0, may hold values from 0.05 to 0.8
Outputs:
- layer_out: bfloat16 [3072, 2048], P(('grp', 'ep'), 'tp'), parts along dimension 0
- new_state: float32 [2, 3072, 4096], P(None, ('grp', 'ep'), 'tp'), parts along dimension 1
There are 2 independent parts, one for each index of `grp`. A program takes and returns all parts, laid end to end along the dimension named above; an argument that names none is the same for every part. Nothing has to cross between parts.
Inputs may be any that keep to these rules, and one draw needn't show every extreme that they name: `routes`: each row names 6 different experts; among the rows of one index of ep no expert is named by more than 54 rows.
All inputs are finite; a program needn't handle non-finite values.
Results may differ from a plain program's by a relative error of at most 0.017.
Values may be sent and summed in bfloat16 or wider, within the bound.
A program may use at most 128 MiB of HBM per device.

v0:
```python
import functools
import jax
import jax.numpy as jnp
from jax import lax
from jax.experimental import pallas as pl
from jax.experimental.pallas import tpu as pltpu
from jax.sharding import PartitionSpec as P

norm_eps = 1e-06
highest = lax.Precision.HIGHEST
MESH = pl.DeviceIdType.MESH


def root_scale(activations, scale_gain):
    values = activations.astype(jnp.float32)
    factor = lax.rsqrt(jnp.mean(values * values, axis=-1, keepdims=True) + norm_eps)
    return (values * factor * scale_gain).astype(jnp.bfloat16)


def state_update(
    drive_rows, prior_state, decay_rate, frequency, log_step, input_map, output_map, skip_gain
):
    sequences = drive_rows.shape[0]
    groups = decay_rate.shape[0]
    driven = drive_rows.astype(jnp.float32).reshape(sequences, groups, -1)
    step_size = jnp.exp(log_step)[:, None]
    real_rate = -decay_rate
    magnitude = jnp.exp(real_rate * step_size)
    turn_real = magnitude * jnp.cos(frequency * step_size)
    turn_imag = magnitude * jnp.sin(frequency * step_size)
    denominator = real_rate * real_rate + frequency * frequency
    hold_real = ((turn_real - 1.0) * real_rate + turn_imag * frequency) / denominator
    hold_imag = (turn_imag * real_rate - (turn_real - 1.0) * frequency) / denominator
    push_real = jnp.einsum("sgh,gph->sgp", driven, input_map[0], precision=highest)
    push_imag = jnp.einsum("sgh,gph->sgp", driven, input_map[1], precision=highest)
    enter_real = push_real * hold_real - push_imag * hold_imag
    enter_imag = push_real * hold_imag + push_imag * hold_real
    old_real = prior_state[0].reshape(sequences, groups, -1)
    old_imag = prior_state[1].reshape(sequences, groups, -1)
    fresh_real = turn_real * old_real - turn_imag * old_imag + enter_real
    fresh_imag = turn_real * old_imag + turn_imag * old_real + enter_imag
    readout = jnp.einsum("ghp,sgp->sgh", output_map[0], fresh_real, precision=highest)
    readout = readout - jnp.einsum("ghp,sgp->sgh", output_map[1], fresh_imag, precision=highest)
    readout = readout.reshape(sequences, -1) + skip_gain * drive_rows.astype(jnp.float32)
    fresh = jnp.stack([fresh_real.reshape(sequences, -1), fresh_imag.reshape(sequences, -1)])
    return (readout, fresh)


def exchanged_experts(second_normed, routes, route_weights, expert_gate, expert_up, expert_down):
    experts = lax.axis_size("ep")
    seq_rows, top_count = routes.shape
    slot_cap = min(seq_rows, max(2, 3 * seq_rows * top_count // (2 * experts)))
    flat_routes = routes.reshape(-1)
    one_hot = (flat_routes[:, None] == jnp.arange(experts, dtype=jnp.int32)[None, :]).astype(
        jnp.int32
    )
    ranked = jnp.sum((jnp.cumsum(one_hot, axis=0) - one_hot) * one_hot, axis=1)
    slot_index = flat_routes * slot_cap + ranked
    placed = slot_index[:, None] == jnp.arange(experts * slot_cap, dtype=jnp.int32)[None, :]
    placed_rows = jnp.any(placed.reshape(seq_rows, top_count, experts * slot_cap), axis=1).astype(
        jnp.bfloat16
    )
    outgoing = lax.dot_general(
        placed_rows, second_normed, (((0,), (0,)), ((), ())), preferred_element_type=jnp.float32
    ).astype(jnp.bfloat16)
    outgoing = outgoing.reshape(experts, slot_cap, -1)
    arrived = lax.all_to_all(outgoing, "ep", split_axis=0, concat_axis=0, tiled=True)
    sources, count_items, full_width = arrived.shape
    expert_rows = arrived.reshape(sources * count_items, full_width)
    gate_val = jnp.dot(expert_rows, expert_gate[0], preferred_element_type=jnp.float32)
    up_val = jnp.dot(expert_rows, expert_up[0], preferred_element_type=jnp.float32)
    hidden = (jax.nn.silu(gate_val) * up_val).astype(jnp.bfloat16)
    piece = jnp.dot(hidden, expert_down[0], preferred_element_type=jnp.float32)
    summed = lax.psum_scatter(
        piece.reshape(sources, count_items, full_width).astype(jnp.bfloat16),
        "tp",
        scatter_dimension=2,
        tiled=True,
    )
    returned = lax.all_to_all(summed, "ep", split_axis=0, concat_axis=0, tiled=True)
    flat_back = returned.reshape(experts * slot_cap, -1)
    picked = (
        jnp.take(flat_back, slot_index, axis=0).reshape(seq_rows, top_count, -1).astype(jnp.float32)
    )
    routed = jnp.einsum("sk,skd->sd", route_weights, picked)
    return routed


def near_first(extent):
    return [sorted(range(extent), key=lambda other: (abs(other - at), min(other, extent - 1 - other))) for at in range(extent)]


def looked_up(table, position):
    found = jnp.int32(0)
    for at, entry in enumerate(table):
        found = jnp.where(position == at, jnp.int32(entry), found)
    return found


def expert_kernel(
    grid_shape, pieces,
    own, middle, weights, gate_in, up_in, down_in, sgate_in, sup_in, sdown_in,
    out,
    rows_all, back, from_twin, from_side, from_far, weight_all,
    gate, up, down, sgate, sup, sdown, hidden, shared, total,
    load_sem, row_recv, own_z_send, fwd_z_send, fwd_x_send, fwd_twin_send,
    w_send, w_recv, twin_send, twin_recv, side_send, side_recv, far_send, far_recv,
):
    zs, xs, cs = grid_shape
    count = zs * xs * cs
    me = lax.axis_index("ep")
    core = lax.rem(me, cs)
    col = lax.rem(me // cs, xs)
    level = me // (cs * xs)
    rows, width = own.shape
    span = rows // pieces
    hid = gate.shape[1]

    def device(z, x, c):
        return (z * xs + x) * cs + c

    twin = device(level, col, 1 - core)
    side = device(level, 1 - col, core)
    order = [looked_up([row[j] for row in near_first(zs)], level) for j in range(zs)]

    def part(base, h):
        return pl.ds(pl.multiple_of(base * rows + h * span, 16), span)

    loads = [
        pltpu.make_async_copy(src, dst, load_sem.at[n])
        for n, (src, dst) in enumerate(
            ((gate_in.at[0], gate), (up_in.at[0], up), (down_in.at[0], down),
             (sgate_in, sgate), (sup_in, sup), (sdown_in, sdown))
        )
    ]
    for load in loads:
        load.start()

    barrier = pltpu.get_barrier_semaphore()
    for step in range(1, count):
        pl.semaphore_signal(
            barrier, inc=1, device_id={"ep": lax.rem(me + step, count)}, device_id_type=MESH
        )
    pl.semaphore_wait(barrier, count - 1)

    def remote(src, dst, send, recv, target):
        return pltpu.make_async_remote_copy(
            src_ref=src, dst_ref=dst, send_sem=send, recv_sem=recv,
            device_id={"ep": target}, device_id_type=MESH,
        )

    sent = []

    def push(src, dst, send, recv, target):
        copy = remote(src, dst, send, recv, target)
        copy.start()
        sent.append(copy)

    def row_copy(src_ref, src_rows, origin, h, send, target):
        return remote(
            src_ref.at[src_rows], rows_all.at[part(origin, h)], send, row_recv.at[origin, h], target
        )

    for h in range(pieces):
        piece = pl.ds(h * span, span)

        @pl.when(level > 0)
        def _():
            row_copy(own, piece, me, h, own_z_send.at[0, h], device(level - 1, col, core)).start()

        @pl.when(level < zs - 1)
        def _():
            row_copy(own, piece, me, h, own_z_send.at[1, h], device(level + 1, col, core)).start()

        for send, target in ((fwd_x_send.at[0, h], side), (fwd_twin_send.at[0, h], twin)):
            copy = row_copy(own, piece, me, h, send, target)
            copy.start()
            sent.append(copy)

    for step in range(1, count):
        other = lax.rem(me + step, count)
        push(
            weights.at[other], weight_all.at[me], w_send.at[step], w_recv.at[count - step], other
        )
    rows_all[part(me, 0), :] = own[pl.ds(0, span), :]
    for h in range(1, pieces):
        rows_all[part(me, h), :] = own[pl.ds(h * span, span), :]
    weight_all[me] = weights[me]

    def arrived(origin, h):
        row_copy(own, pl.ds(h * span, span), origin, h, own_z_send.at[0, h], twin).wait_recv()

    def feed(source, take, gate_w, up_w, down_w, finish):
        def first(n, carry):
            cols = pl.ds(pl.multiple_of(n * 256, 256), 256)
            data = source()
            g = jnp.dot(data, gate_w[:, cols], preferred_element_type=jnp.float32)
            u = jnp.dot(data, up_w[:, cols], preferred_element_type=jnp.float32)
            hidden[pl.ds(0, take), cols] = (jax.nn.silu(g) * u).astype(jnp.bfloat16)
            return carry

        lax.fori_loop(0, hid // 256, first, 0)

        def second(n, carry):
            cols = pl.ds(pl.multiple_of(n * 512, 512), 512)
            piece = jnp.dot(
                hidden[pl.ds(0, take), :], down_w[:, cols], preferred_element_type=jnp.float32
            )
            finish(cols, piece.astype(jnp.bfloat16))
            return carry

        lax.fori_loop(0, width // 512, second, 0)

    def chip(label, z, x):
        base = device(z, x, 0)
        block = pl.ds(pl.multiple_of(base * rows, 16), cs * rows)
        scales = []
        for c in range(cs):
            line = jnp.broadcast_to(weight_all[base + c], (128, 128))
            scales.append(jnp.transpose(line)[:rows])
        scale = jnp.concatenate(scales, axis=0)
        scale = jnp.concatenate([scale] * 4, axis=1)

        def finish(cols, piece):
            back[block, cols] = (piece.astype(jnp.float32) * scale).astype(jnp.bfloat16)

        feed(lambda: rows_all[block, :], cs * rows, gate, up, down, finish)
        push(
            back.at[part_all(device(z, x, 1 - core))],
            from_twin.at[label],
            twin_send.at[label],
            twin_recv.at[label],
            twin,
        )

    def part_all(origin):
        return pl.ds(pl.multiple_of(origin * rows, 16), rows)

    def keep(cols, piece):
        shared[:, cols] = piece

    def pair_in(z, x):
        for h in range(pieces):
            arrived(device(z, x, 1 - core), h)

    def onward_of(j):
        return jnp.where(order[j] < level, level + 1, level - 1)

    def fwd_copies(j, h):
        origin = device(order[j], col, core)
        return [
            row_copy(rows_all, part(origin, h), origin, h, send, target)
            for send, target in ((fwd_x_send.at[j, h], side), (fwd_twin_send.at[j, h], twin))
        ]

    def fwd(j):
        for h in range(pieces):
            fwd_piece(j, h)

    def fwd_piece(j, h):
        origin = device(order[j], col, core)
        arrived(origin, h)
        onward = onward_of(j)

        @pl.when((onward >= 0) & (onward < zs))
        def _():
            row_copy(
                rows_all, part(origin, h), origin, h, fwd_z_send.at[j, h],
                device(onward, col, core),
            ).start()

        for copy in fwd_copies(j, h):
            copy.start()

    def across_in(j):
        across = device(order[j], 1 - col, core)
        for h in range(pieces):
            arrived(across, h)
            copy = row_copy(rows_all, part(across, h), across, h, fwd_twin_send.at[zs + j, h], twin)
            copy.start()
            sent.append(copy)

    def own_chip(j):
        pair_in(order[j], col)
        chip(j, order[j], col)

    def across_chip(j):
        pair_in(order[j], 1 - col)
        chip(zs + j, order[j], 1 - col)

    inner = (level > 0) & (level < zs - 1)
    outer = (level == 0) | (level == zs - 1)

    for load in loads[:3]:
        load.wait()
    for step in range(1, count):
        remote(
            weights.at[me], weight_all.at[lax.rem(me + step, count)],
            w_send.at[step], w_recv.at[step], twin,
        ).wait_recv()
    own_chip(0)
    for h in range(pieces):
        fwd_piece(1, h)
        pl.when(inner)(functools.partial(fwd_piece, 2, h))
        if h == 0:
            for load in loads[3:]:
                load.wait()
            feed(lambda: own[...], rows, sgate, sup, sdown, keep)
    across_in(0)
    own_chip(1)
    across_chip(0)
    for h in range(pieces):
        pl.when(inner)(functools.partial(fwd_piece, 3, h))
        pl.when(outer)(functools.partial(fwd_piece, 2, h))
    across_in(1)
    own_chip(2)
    across_chip(1)
    pl.when(outer)(functools.partial(fwd, 3))
    across_in(2)
    own_chip(3)
    across_chip(2)

    def twin_in(label):
        remote(
            from_twin.at[label], from_twin.at[label], twin_send.at[label], twin_recv.at[label], twin
        ).wait_recv()

    def added(first, others, store):
        def strip(n, carry):
            at = pl.multiple_of(n * 16, 16)
            value = first(at).astype(jnp.float32)
            for other in others:
                value = value + other(at).astype(jnp.float32)
            store(at, value)
            return carry

        lax.fori_loop(0, span // 16, strip, 0)

    def back_at(origin, h):
        return lambda at: back[pl.ds(pl.multiple_of(origin * rows + h * span + at, 16), 16), :]

    def slot_at(ref, slot, h):
        return lambda at: ref[slot, pl.ds(pl.multiple_of(h * span + at, 16), 16), :]

    def to_back(origin, h):
        def store(at, value):
            back[pl.ds(pl.multiple_of(origin * rows + h * span + at, 16), 16), :] = value.astype(
                jnp.bfloat16
            )

        return store

    def side_out(j):
        twin_in(zs + j)
        origin = device(order[j], 1 - col, core)
        for h in range(pieces):
            added(back_at(origin, h), [slot_at(from_twin, zs + j, h)], to_back(origin, h))
            push(
                back.at[part(origin, h)], from_side.at[j, pl.ds(h * span, span)],
                side_send.at[j, h], side_recv.at[j, h], side,
            )

    side_out(2)
    across_in(3)
    across_chip(3)
    for j in (3, 1, 0):
        side_out(j)

    def side_in(j, h):
        view = from_side.at[j, pl.ds(h * span, span)]
        remote(view, view, side_send.at[j, h], side_recv.at[j, h], side).wait_recv()

    def far_in(slot, h):
        view = from_far.at[slot, pl.ds(h * span, span)]
        remote(view, view, far_send.at[0, h], far_recv.at[slot, h], side).wait_recv()

    for j in (2, 3, 1):
        twin_in(j)
        goal = order[j]
        origin = device(goal, col, core)
        nearer = jnp.where(goal < level, level - 1, level + 1)
        behind = jnp.where(goal < level, level + 1, level - 1)
        slot = jnp.where((nearer == goal) & (goal > level), zs, goal)
        for h in range(pieces):
            side_in(j, h)
            terms = [slot_at(from_twin, j, h), slot_at(from_side, j, h)]

            @pl.when((behind >= 0) & (behind < zs))
            def _():
                far_in(goal, h)
                added(
                    back_at(origin, h), terms + [slot_at(from_far, goal, h)], to_back(origin, h)
                )

            @pl.when((behind < 0) | (behind >= zs))
            def _():
                added(back_at(origin, h), terms, to_back(origin, h))

            push(
                back.at[part(origin, h)], from_far.at[slot, pl.ds(h * span, span)],
                far_send.at[j, h], far_recv.at[slot, h], device(nearer, col, core),
            )
    twin_in(0)
    for h in range(pieces):
        side_in(0, h)

        def to_total(at, value):
            total[pl.ds(pl.multiple_of(h * span + at, 16), 16), :] = value

        def total_at(at):
            return total[pl.ds(pl.multiple_of(h * span + at, 16), 16), :]

        added(back_at(me, h), [slot_at(from_twin, 0, h), slot_at(from_side, 0, h)], to_total)

        @pl.when(level > 0)
        def _():
            far_in(zs, h)
            added(total_at, [slot_at(from_far, zs, h)], to_total)

        @pl.when(level < zs - 1)
        def _():
            far_in(level, h)
            added(total_at, [slot_at(from_far, level, h)], to_total)

        def plain(ref):
            return lambda at: ref[pl.ds(pl.multiple_of(h * span + at, 16), 16), :]

        def to_out(at, value):
            out[pl.ds(pl.multiple_of(h * span + at, 16), 16), :] = value.astype(jnp.bfloat16)

        added(plain(middle), [total_at, plain(shared)], to_out)

    for copy in sent:
        copy.wait_send()
    for h in range(pieces):
        piece = pl.ds(h * span, span)

        @pl.when(level > 0)
        def _():
            row_copy(own, piece, me, h, own_z_send.at[0, h], twin).wait_send()

        @pl.when(level < zs - 1)
        def _():
            row_copy(own, piece, me, h, own_z_send.at[1, h], twin).wait_send()

        for j in range(1, zs):
            for copy in fwd_copies(j, h):
                copy.wait_send()
            onward = onward_of(j)

            @pl.when((onward >= 0) & (onward < zs))
            def _():
                row_copy(own, piece, me, h, fwd_z_send.at[j, h], twin).wait_send()


def expert_stage(
    second_normed, middle, routes, route_weights,
    expert_gate, expert_up, expert_down, shared_gate, shared_up, shared_down,
):
    experts = lax.axis_size("ep")
    grid_shape = (experts // 4, 2, 2)
    zs = grid_shape[0]
    rows, width = second_normed.shape
    hid = expert_gate.shape[2]
    pieces = 3 if rows % 48 == 0 else 1
    chosen = routes[None, :, :] == jnp.arange(experts, dtype=jnp.int32)[:, None, None]
    weights = jnp.sum(jnp.where(chosen, route_weights[None], 0.0), axis=2)
    weights = jnp.pad(weights, ((0, 0), (0, 128 - rows)))[:, None, :]
    vmem = pl.BlockSpec(memory_space=pltpu.VMEM)
    hbm = pl.BlockSpec(memory_space=pl.ANY)
    dma = pltpu.SemaphoreType.DMA
    half = jnp.bfloat16
    return pl.pallas_call(
        functools.partial(expert_kernel, grid_shape, pieces),
        out_shape=jax.ShapeDtypeStruct((rows, width), half),
        in_specs=[vmem] * 3 + [hbm] * 6,
        out_specs=vmem,
        scratch_shapes=[
            pltpu.VMEM((experts * rows, width), half),
            pltpu.VMEM((experts * rows, width), half),
            pltpu.VMEM((2 * zs, rows, width), half),
            pltpu.VMEM((zs, rows, width), half),
            pltpu.VMEM((zs + 1, rows, width), half),
            pltpu.VMEM((experts, 1, 128), jnp.float32),
            pltpu.VMEM((width, hid), half),
            pltpu.VMEM((width, hid), half),
            pltpu.VMEM((hid, width), half),
            pltpu.VMEM(shared_gate.shape, half),
            pltpu.VMEM(shared_up.shape, half),
            pltpu.VMEM(shared_down.shape, half),
            pltpu.VMEM((2 * rows, hid), half),
            pltpu.VMEM((rows, width), half),
            pltpu.VMEM((rows, width), jnp.float32),
            dma((6,)),
            dma((experts, pieces)),
            dma((2, pieces)),
            dma((zs, pieces)),
            dma((zs, pieces)),
            dma((2 * zs, pieces)),
            dma((experts,)),
            dma((experts,)),
            dma((2 * zs,)),
            dma((2 * zs,)),
            dma((zs, pieces)),
            dma((zs, pieces)),
            dma((zs, pieces)),
            dma((zs + 1, pieces)),
        ],
        compiler_params=pltpu.CompilerParams(
            collective_id=0, has_side_effects=True, vmem_limit_bytes=60 * 1024 * 1024
        ),
    )(
        second_normed, middle, weights,
        expert_gate, expert_up, expert_down, shared_gate, shared_up, shared_down,
    )


def mixer_kernel(
    tokens, prior, mix_gain, in_weight, params, input_map, output_map, skip, out_weight,
    channel_gain, new_state, middle, second, normed, acts, acc,
):
    step = pl.program_id(0)
    lane = 128
    channels = in_weight.shape[1]
    width = input_map.shape[2]
    group = acts.shape[1] * width // prior.shape[2]
    per = lane // group
    states = per * width

    def scaled(values, gain):
        factor = lax.rsqrt(jnp.mean(values * values, axis=-1, keepdims=True) + norm_eps)
        return (values * factor * gain[...]).astype(jnp.bfloat16)

    @pl.when(step == 0)
    def _():
        normed[...] = scaled(tokens[...].astype(jnp.float32), mix_gain)
        acc[...] = jnp.zeros_like(acc)

    drive = jnp.dot(normed[...], in_weight[...], preferred_element_type=jnp.float32)
    drive = drive.astype(jnp.bfloat16)
    row = lax.broadcasted_iota(jnp.int32, (lane, states), 0) // group
    column = lax.broadcasted_iota(jnp.int32, (lane, states), 1) // width
    own_group = row == column

    def spread(table):
        tiled = jnp.concatenate([table] * per, axis=1)
        return jnp.where(own_group, tiled, 0.0).astype(jnp.bfloat16)

    for sub in range(channels // lane):
        cols = slice(sub * lane, (sub + 1) * lane)
        ent = slice(sub * states, (sub + 1) * states)
        part = drive[:, cols]
        push_real = jnp.dot(
            part, spread(input_map[0, cols, :]), preferred_element_type=jnp.float32
        )
        push_imag = jnp.dot(
            part, spread(input_map[1, cols, :]), preferred_element_type=jnp.float32
        )
        turn_real, turn_imag = params[0:1, ent], params[1:2, ent]
        hold_real, hold_imag = params[2:3, ent], params[3:4, ent]
        old_real, old_imag = prior[0, :, ent], prior[1, :, ent]
        fresh_real = (
            turn_real * old_real - turn_imag * old_imag
            + (push_real * hold_real - push_imag * hold_imag)
        )
        fresh_imag = (
            turn_real * old_imag + turn_imag * old_real
            + (push_real * hold_imag + push_imag * hold_real)
        )
        new_state[0, :, ent] = fresh_real
        new_state[1, :, ent] = fresh_imag
        across = (((1,), (1,)), ((), ()))
        readout = lax.dot_general(
            fresh_real.astype(jnp.bfloat16), spread(output_map[0, cols, :]), across,
            preferred_element_type=jnp.float32,
        ) - lax.dot_general(
            fresh_imag.astype(jnp.bfloat16), spread(output_map[1, cols, :]), across,
            preferred_element_type=jnp.float32,
        )
        readout = readout + skip[:, cols] * part.astype(jnp.float32)
        acts[:, cols] = jax.nn.gelu(readout).astype(jnp.bfloat16)
    acc[...] += jnp.dot(acts[...], out_weight[...], preferred_element_type=jnp.float32)

    @pl.when(step == pl.num_programs(0) - 1)
    def _():
        mixed = acc[...].astype(jnp.bfloat16).astype(jnp.float32)
        mid = (tokens[...].astype(jnp.float32) + mixed).astype(jnp.bfloat16)
        middle[...] = mid
        second[...] = scaled(mid.astype(jnp.float32), channel_gain)


def mixer_stage(
    tokens, prior_state, mix_gain, in_weight, decay_rate, frequency, log_step,
    input_map, output_map, skip_gain, out_weight, channel_gain,
):
    rows, model = tokens.shape
    groups, width = decay_rate.shape
    channels = in_weight.shape[1]
    step_size = jnp.exp(log_step)[:, None]
    real_rate = -decay_rate
    magnitude = jnp.exp(real_rate * step_size)
    turn_real = magnitude * jnp.cos(frequency * step_size)
    turn_imag = magnitude * jnp.sin(frequency * step_size)
    denominator = real_rate * real_rate + frequency * frequency
    hold_real = ((turn_real - 1.0) * real_rate + turn_imag * frequency) / denominator
    hold_imag = (turn_imag * real_rate - (turn_real - 1.0) * frequency) / denominator
    params = jnp.stack([turn_real, turn_imag, hold_real, hold_imag]).reshape(4, -1)
    in_map = jnp.transpose(input_map, (0, 1, 3, 2)).reshape(2, channels, width)
    out_map = output_map.reshape(2, channels, width)
    block = 256
    states = block * groups * width // channels

    def whole(*shape):
        return pl.BlockSpec(shape, lambda i: (0,) * len(shape))

    half = jnp.bfloat16
    return pl.pallas_call(
        mixer_kernel,
        grid=(channels // block,),
        out_shape=(
            jax.ShapeDtypeStruct(prior_state.shape, jnp.float32),
            jax.ShapeDtypeStruct((rows, model), half),
            jax.ShapeDtypeStruct((rows, model), half),
        ),
        in_specs=[
            whole(rows, model),
            pl.BlockSpec((2, rows, states), lambda i: (0, 0, i)),
            whole(1, model),
            pl.BlockSpec((model, block), lambda i: (0, i)),
            pl.BlockSpec((4, states), lambda i: (0, i)),
            pl.BlockSpec((2, block, width), lambda i: (0, i, 0)),
            pl.BlockSpec((2, block, width), lambda i: (0, i, 0)),
            pl.BlockSpec((1, block), lambda i: (0, i)),
            pl.BlockSpec((block, model), lambda i: (i, 0)),
            whole(1, model),
        ],
        out_specs=(
            pl.BlockSpec((2, rows, states), lambda i: (0, 0, i)),
            whole(rows, model),
            whole(rows, model),
        ),
        scratch_shapes=[
            pltpu.VMEM((rows, model), half),
            pltpu.VMEM((rows, block), half),
            pltpu.VMEM((rows, model), jnp.float32),
        ],
        compiler_params=pltpu.CompilerParams(
            dimension_semantics=("arbitrary",), vmem_limit_bytes=62 * 1024 * 1024
        ),
    )(
        tokens, prior_state, mix_gain[None], in_weight, params, in_map, out_map,
        skip_gain[None], out_weight, channel_gain[None],
    )


def body(
    tokens,
    prior_state,
    mix_gain,
    in_weight,
    decay_rate,
    frequency,
    log_step,
    input_map,
    output_map,
    skip_gain,
    out_weight,
    channel_gain,
    expert_gate,
    expert_up,
    expert_down,
    shared_gate,
    shared_up,
    shared_down,
    routes,
    route_weights,
):
    if lax.axis_size("tp") == 1 and lax.axis_size("ep") == 16:
        new_state, middle, second_normed = mixer_stage(
            tokens, prior_state, mix_gain, in_weight, decay_rate, frequency, log_step,
            input_map, output_map, skip_gain, out_weight, channel_gain,
        )
        layer_out = expert_stage(
            second_normed, middle, routes, route_weights,
            expert_gate, expert_up, expert_down, shared_gate, shared_up, shared_down,
        )
        return (layer_out, new_state)
    normed = root_scale(tokens, mix_gain)
    drive_rows = jnp.dot(normed, in_weight, preferred_element_type=jnp.float32).astype(jnp.bfloat16)
    readout, new_state = state_update(
        drive_rows, prior_state, decay_rate, frequency, log_step, input_map, output_map, skip_gain
    )
    activated = jax.nn.gelu(readout).astype(jnp.bfloat16)
    partial_value = jnp.dot(activated, out_weight, preferred_element_type=jnp.float32)
    mixer_out = lax.psum(partial_value.astype(jnp.bfloat16), "tp").astype(jnp.float32)
    middle = (tokens.astype(jnp.float32) + mixer_out).astype(jnp.bfloat16)
    second_normed = root_scale(middle, channel_gain)
    shared_gval = jnp.dot(second_normed, shared_gate, preferred_element_type=jnp.float32)
    shared_uval = jnp.dot(second_normed, shared_up, preferred_element_type=jnp.float32)
    shared_hidden = (jax.nn.silu(shared_gval) * shared_uval).astype(jnp.bfloat16)
    shared_piece = jnp.dot(shared_hidden, shared_down, preferred_element_type=jnp.float32)
    shared_out = lax.psum_scatter(
        shared_piece.astype(jnp.bfloat16), "tp", scatter_dimension=1, tiled=True
    ).astype(jnp.float32)
    half_cols = second_normed.shape[1] // lax.axis_size("tp")
    routed = exchanged_experts(
        second_normed, routes, route_weights, expert_gate, expert_up, expert_down
    )
    own_middle = lax.dynamic_slice_in_dim(middle, lax.axis_index("tp") * half_cols, half_cols, 1)
    layer_out = (own_middle.astype(jnp.float32) + routed + shared_out).astype(jnp.bfloat16)
    return (layer_out, new_state)


def solution(mesh):
    in_specs = (
        P(("grp", "ep"), None),
        P(None, ("grp", "ep"), "tp"),
        P(),
        P(None, "tp"),
        P("tp", None),
        P("tp", None),
        P("tp"),
        P(None, "tp", None, None),
        P(None, "tp", None, None),
        P("tp"),
        P("tp", None),
        P(),
        P("ep", None, "tp"),
        P("ep", None, "tp"),
        P("ep", "tp", None),
        P(None, "tp"),
        P(None, "tp"),
        P("tp", None),
        P(("grp", "ep"), None),
        P(("grp", "ep"), None),
    )
    out_specs = (P(("grp", "ep"), "tp"), P(None, ("grp", "ep"), "tp"))
    return jax.shard_map(body, mesh=mesh, in_specs=in_specs, out_specs=out_specs, check_vma=False)
```

profile of v0, /device:TPU:0, one launch (start us, length us, event | category | flops | bytes accessed | tf_op | source)
XLA Modules:
  0.0 101.9 jit_solution(5469589380774440581)
XLA Ops:
  0.6 0.7 exp.6
  1.3 0.7 select_reduce_fusion
  2.0 0.6 pad.4
  2.6 1.0 cosine_multiply_fusion
  3.6 0.1 stack.15
  3.7 0.1 stack.17
  3.8 0.1 stack.18
  3.9 0.1 stack.16
  4.0 0.7 pad_maximum_fusion.params
  4.7 10.4 %shard_map.203 = (f32[2,96,4096]{2,1,0:T(8,128)}, bf16[96,2048]{1,0:T(8,128)(2,1)}, bf16[96,2048]{1,0:T(8,128)(2,1)}) custom-call(bf16[96,2048]{1,0:T(8,128)(2,1)} %tokens.1, f32[2,96,4096]{2,1,0:T(8,128)} %prior.1, f32[1,2048]{1,0:T(1,128)} %bitcast.11, bf16[2048,1024]{1,0:T(8,128)(2,1)} %in_weight.1, f32[4,4096]{1,0:T(4,128)} %pad_maximum_fusion.params, ...), custom_call_target="tpu_custom_call" | custom-call | tf_op jit(solution)/shard_map/pallas_call | solution.py:617
  15.0 85.1 %shard_map.204 = bf16[96,2048]{1,0:T(8,128)(2,1)} custom-call(bf16[96,2048]{1,0:T(8,128)(2,1)} %get-tuple-element.5.own, bf16[96,2048]{1,0:T(8,128)(2,1)} %get-tuple-element.6.middle, f32[16,1,128]{2,1,0:T(1,128)} %bitcast.10, bf16[1,2048,512]{2,1,0:T(8,128)(2,1)} %gate_in.1, bf16[1,2048,512]{2,1,0:T(8,128)(2,1)} %up_in.1, bf16[1,512,2048]{2,1,0:T(8,128)(2,1)} %down_in.1, ...), custom_call_target="tpu_custom_call" | custom-call | tf_op jit(solution)/shard_map/pallas_call | solution.py:473
  100.2 1.8 %copy.25 = bf16[96,2048]{1,0:T(8,128)(2,1)} copy(bf16[96,2048]{1,0:T(8,128)(2,1)} %shard_map.204) | data formatting | bytes 786432
where the time goes:
time: 102 us
  Pallas kernels  95.5 us (94%)
  local copies, waits for them, and re-layouts  3.36 us (3%)
  other arithmetic  2.4 us (2%)
    pallas_call x1, Pallas kernels, expert_stage(): pl.pallas_call(functools.partial(expert_kernel, grid_shape, pieces), out_...  85.1 us
    pallas_call x1, Pallas kernels, mixer_stage(): pl.pallas_call(mixer_kernel, grid=(channels // block,), out_shape=(jax.Sh...  10.4 us

commit v1 on v0

v1 whole, which is shorter than its diff:
```python
import functools
import jax
import jax.numpy as jnp
from jax import lax
from jax.experimental import pallas as pl
from jax.experimental.pallas import tpu as pltpu
from jax.sharding import PartitionSpec as P

norm_eps = 1e-06
highest = lax.Precision.HIGHEST
MESH = pl.DeviceIdType.MESH


def root_scale(activations, scale_gain):
    values = activations.astype(jnp.float32)
    factor = lax.rsqrt(jnp.mean(values * values, axis=-1, keepdims=True) + norm_eps)
    return (values * factor * scale_gain).astype(jnp.bfloat16)


def state_update(
    drive_rows, prior_state, decay_rate, frequency, log_step, input_map, output_map, skip_gain
):
    sequences = drive_rows.shape[0]
    groups = decay_rate.shape[0]
    driven = drive_rows.astype(jnp.float32).reshape(sequences, groups, -1)
    step_size = jnp.exp(log_step)[:, None]
    real_rate = -decay_rate
    magnitude = jnp.exp(real_rate * step_size)
    turn_real = magnitude * jnp.cos(frequency * step_size)
    turn_imag = magnitude * jnp.sin(frequency * step_size)
    denominator = real_rate * real_rate + frequency * frequency
    hold_real = ((turn_real - 1.0) * real_rate + turn_imag * frequency) / denominator
    hold_imag = (turn_imag * real_rate - (turn_real - 1.0) * frequency) / denominator
    push_real = jnp.einsum("sgh,gph->sgp", driven, input_map[0], precision=highest)
    push_imag = jnp.einsum("sgh,gph->sgp", driven, input_map[1], precision=highest)
    enter_real = push_real * hold_real - push_imag * hold_imag
    enter_imag = push_real * hold_imag + push_imag * hold_real
    old_real = prior_state[0].reshape(sequences, groups, -1)
    old_imag = prior_state[1].reshape(sequences, groups, -1)
    fresh_real = turn_real * old_real - turn_imag * old_imag + enter_real
    fresh_imag = turn_real * old_imag + turn_imag * old_real + enter_imag
    readout = jnp.einsum("ghp,sgp->sgh", output_map[0], fresh_real, precision=highest)
    readout = readout - jnp.einsum("ghp,sgp->sgh", output_map[1], fresh_imag, precision=highest)
    readout = readout.reshape(sequences, -1) + skip_gain * drive_rows.astype(jnp.float32)
    fresh = jnp.stack([fresh_real.reshape(sequences, -1), fresh_imag.reshape(sequences, -1)])
    return (readout, fresh)


def exchanged_experts(second_normed, routes, route_weights, expert_gate, expert_up, expert_down):
    experts = lax.axis_size("ep")
    seq_rows, top_count = routes.shape
    slot_cap = min(seq_rows, max(2, 3 * seq_rows * top_count // (2 * experts)))
    flat_routes = routes.reshape(-1)
    one_hot = (flat_routes[:, None] == jnp.arange(experts, dtype=jnp.int32)[None, :]).astype(
        jnp.int32
    )
    ranked = jnp.sum((jnp.cumsum(one_hot, axis=0) - one_hot) * one_hot, axis=1)
    slot_index = flat_routes * slot_cap + ranked
    placed = slot_index[:, None] == jnp.arange(experts * slot_cap, dtype=jnp.int32)[None, :]
    placed_rows = jnp.any(placed.reshape(seq_rows, top_count, experts * slot_cap), axis=1).astype(
        jnp.bfloat16
    )
    outgoing = lax.dot_general(
        placed_rows, second_normed, (((0,), (0,)), ((), ())), preferred_element_type=jnp.float32
    ).astype(jnp.bfloat16)
    outgoing = outgoing.reshape(experts, slot_cap, -1)
    arrived = lax.all_to_all(outgoing, "ep", split_axis=0, concat_axis=0, tiled=True)
    sources, count_items, full_width = arrived.shape
    expert_rows = arrived.reshape(sources * count_items, full_width)
    gate_val = jnp.dot(expert_rows, expert_gate[0], preferred_element_type=jnp.float32)
    up_val = jnp.dot(expert_rows, expert_up[0], preferred_element_type=jnp.float32)
    hidden = (jax.nn.silu(gate_val) * up_val).astype(jnp.bfloat16)
    piece = jnp.dot(hidden, expert_down[0], preferred_element_type=jnp.float32)
    summed = lax.psum_scatter(
        piece.reshape(sources, count_items, full_width).astype(jnp.bfloat16),
        "tp",
        scatter_dimension=2,
        tiled=True,
    )
    returned = lax.all_to_all(summed, "ep", split_axis=0, concat_axis=0, tiled=True)
    flat_back = returned.reshape(experts * slot_cap, -1)
    picked = (
        jnp.take(flat_back, slot_index, axis=0).reshape(seq_rows, top_count, -1).astype(jnp.float32)
    )
    routed = jnp.einsum("sk,skd->sd", route_weights, picked)
    return routed


PIECES = (
    (1, 0, 1, 0, 8),
    (0, 1, 1, 0, 8),
    (1, 2, 1, 0, 8),
    (0, 3, 1, 0, 8),
    (0, 4, 1, 0, 8),
    (0, 5, 1, 0, 5),
    (1, 5, 1, 5, 3),
)

END_PROGRAM = (
    (0, 0, 0, 0, 2), (0, 0, 0, 0, 0), (0, 0, 0, 1, 2), (0, 0, 0, 1, 0), (0, 0, 0, 3, 2),
    (0, 0, 0, 2, 2), (0, 0, 0, 3, 0), (5,), (0, 0, 1, 0, 0), (0, 0, 0, 2, 0), (0, 0, 0, 4, 0),
    (0, 1, 0, 1, 2), (0, 1, 0, 3, 2), (0, 0, 0, 4, 2), (0, 0, 1, 2, 0), (0, 0, 0, 5, 0),
    (0, 0, 0, 6, 0), (3, ((0, (0,)),)), (0, 2, 0, 1, 2), (0, 0, 0, 5, 2), (0, 0, 0, 6, 2),
    (3, ((1, (0,)),)), (4, ((0, (0,)),)), (1, 0, 1, 1, 2), (4, ((1, (0,)),)), (1, 1, 0, 0, 0),
    (1, 1, 1, 0, 0), (0, 3, 0, 1, 2), (1, 1, 1, 1, 2), (0, 0, 1, 6, 0), (3, ((2, (0,)),)),
    (4, ((2, (0,)),)), (1, 2, 0, 0, 0), (1, 2, 1, 0, 0), (1, 2, 1, 1, 2), (0, 3, 0, 3, 2),
    (3, ((3, (0,)),)), (0, 2, 0, 3, 2), (4, ((3, (0,)),)), (1, 3, 0, 0, 0), (1, 3, 1, 0, 0),
    (1, 3, 1, 1, 2), (1, 2, 0, 1, 0), (1, 1, 0, 1, 0), (3, ((2, (1,)), (3, (1,)))),
    (1, 3, 0, 1, 0), (4, ((2, (1,)), (3, (1,)))), (0, 3, 0, 4, 2), (1, 3, 0, 2, 0),
    (1, 3, 1, 2, 0), (1, 3, 1, 3, 2), (1, 2, 0, 2, 0), (1, 2, 1, 2, 0), (1, 2, 1, 3, 2),
    (0, 3, 0, 5, 2), (3, ((1, (1,)),)), (4, ((1, (1,)),)), (0, 2, 0, 4, 2), (1, 3, 0, 3, 0),
    (1, 1, 1, 3, 2), (0, 2, 0, 5, 2), (1, 2, 0, 3, 0), (1, 1, 0, 2, 0), (1, 1, 1, 2, 0),
    (0, 1, 0, 4, 2), (0, 1, 0, 5, 2), (3, ((0, (1,)), (3, (2,)))), (4, ((0, (1,)), (3, (2,)))),
    (1, 3, 0, 6, 0), (1, 3, 1, 4, 2), (1, 3, 1, 5, 2), (1, 3, 1, 6, 0), (1, 1, 0, 3, 0),
    (3, ((2, (2,)),)), (4, ((2, (2,)),)), (1, 2, 0, 6, 0), (1, 2, 1, 4, 2), (1, 2, 1, 5, 2),
    (1, 0, 1, 0, 2), (3, ((0, (2,)), (1, (2,)))), (1, 3, 0, 4, 0), (4, ((0, (2,)), (1, (2,)))),
    (1, 3, 0, 5, 0), (1, 2, 1, 6, 0), (1, 1, 1, 4, 2), (1, 1, 1, 5, 2), (2, 0, 0, 1),
    (1, 2, 0, 4, 0), (1, 2, 0, 5, 0), (1, 1, 0, 6, 0), (1, 1, 1, 6, 0), (1, 0, 1, 2, 2),
    (1, 0, 1, 3, 2), (2, 0, 0, 0), (1, 1, 0, 4, 0), (1, 1, 0, 5, 0), (1, 0, 1, 6, 2),
    (1, 0, 1, 4, 2), (1, 0, 1, 5, 2), (2, 0, 0, 2), (2, 0, 0, 3), (2, 0, 0, 6), (2, 0, 0, 4),
    (2, 0, 0, 5),
)

MID_PROGRAM = (
    (0, 1, 0, 0, 2), (0, 1, 0, 0, 0), (0, 1, 0, 0, 1), (0, 1, 0, 1, 2), (0, 1, 0, 1, 0),
    (0, 1, 0, 1, 1), (0, 1, 0, 3, 2), (0, 1, 0, 2, 2), (0, 1, 0, 3, 0), (0, 1, 0, 3, 1), (5,),
    (0, 0, 0, 0, 0), (0, 2, 0, 0, 1), (0, 0, 0, 1, 2), (0, 0, 0, 1, 0), (0, 1, 1, 0, 0),
    (0, 2, 0, 1, 2), (0, 2, 0, 1, 1), (0, 1, 1, 0, 1), (0, 0, 0, 3, 2), (0, 0, 1, 0, 0),
    (0, 0, 0, 3, 0), (0, 3, 0, 0, 1), (3, ((1, (0,)),)), (0, 0, 0, 2, 0), (0, 3, 0, 1, 2),
    (0, 2, 0, 3, 2), (0, 3, 0, 1, 1), (0, 2, 1, 0, 1), (4, ((1, (0,)),)), (1, 1, 1, 1, 2),
    (0, 0, 1, 2, 0), (0, 1, 0, 2, 0), (0, 1, 1, 2, 0), (0, 0, 0, 4, 0), (0, 3, 1, 0, 1),
    (0, 0, 0, 5, 0), (0, 1, 0, 4, 0), (0, 1, 0, 5, 0), (0, 0, 0, 6, 0), (0, 3, 0, 3, 2),
    (0, 0, 0, 4, 2), (0, 0, 0, 5, 2), (0, 1, 0, 4, 2), (0, 1, 0, 5, 2), (0, 1, 0, 6, 2),
    (0, 3, 0, 3, 1), (0, 2, 0, 3, 1), (0, 3, 0, 2, 1), (0, 3, 1, 2, 1), (0, 2, 0, 2, 1),
    (0, 2, 1, 2, 1), (0, 0, 1, 6, 0), (0, 1, 0, 6, 0), (0, 3, 0, 4, 2), (0, 3, 0, 4, 1),
    (0, 3, 0, 5, 2), (0, 3, 0, 5, 1), (0, 1, 0, 2, 1), (0, 1, 1, 2, 1), (0, 2, 0, 4, 2),
    (0, 2, 0, 4, 1), (0, 1, 1, 6, 0), (3, ((0, (1,)), (1, (1, 2)), (2, (0,)))), (0, 2, 0, 5, 2),
    (0, 2, 0, 5, 1), (0, 1, 0, 4, 1), (0, 1, 0, 5, 1), (0, 3, 0, 6, 1), (0, 3, 1, 6, 1),
    (0, 2, 0, 6, 1), (4, ((0, (1,)), (1, (1, 2)), (2, (0,)))), (0, 2, 1, 6, 1), (1, 0, 1, 3, 2),
    (1, 2, 0, 0, 0), (1, 2, 1, 0, 0), (1, 2, 1, 1, 2), (1, 1, 1, 3, 2),
    (3, ((0, (0,)), (3, (0, 2)))), (4, ((0, (0,)), (3, (0, 2)))), (1, 3, 0, 0, 0),
    (1, 3, 1, 0, 0), (1, 3, 1, 1, 2), (1, 3, 1, 4, 2), (3, ((0, (2,)), (2, (1, 2)), (3, (1,)))),
    (1, 2, 0, 1, 0), (4, ((0, (2,)), (2, (1, 2)), (3, (1,)))), (1, 3, 0, 2, 0), (1, 3, 1, 3, 2),
    (1, 3, 1, 5, 2), (1, 0, 1, 1, 2), (1, 0, 0, 0, 1), (1, 2, 1, 3, 2), (1, 1, 1, 0, 2),
    (1, 2, 1, 4, 2), (1, 2, 1, 5, 2), (1, 0, 1, 4, 2), (1, 0, 1, 5, 2), (1, 3, 0, 1, 0),
    (1, 3, 1, 2, 0), (1, 0, 1, 0, 1), (0, 1, 0, 6, 1), (0, 1, 1, 6, 1), (2, 1, 0, 1),
    (1, 3, 0, 3, 0), (1, 2, 0, 2, 0), (1, 2, 1, 2, 0), (1, 0, 0, 2, 1), (1, 0, 0, 1, 1),
    (1, 0, 1, 2, 1), (1, 3, 0, 6, 0), (1, 0, 0, 3, 1), (1, 3, 1, 6, 0), (1, 2, 0, 3, 0),
    (2, 1, 0, 0), (1, 2, 0, 6, 0), (1, 1, 1, 2, 2), (1, 1, 1, 4, 2), (1, 1, 1, 5, 2),
    (1, 0, 0, 6, 1), (1, 3, 0, 4, 0), (1, 0, 1, 6, 1), (1, 3, 0, 5, 0), (1, 2, 1, 6, 0),
    (2, 1, 0, 3), (1, 2, 0, 4, 0), (2, 1, 0, 2), (1, 2, 0, 5, 0), (1, 0, 0, 4, 1),
    (1, 0, 0, 5, 1), (1, 1, 1, 6, 2), (2, 1, 0, 4), (2, 1, 0, 6), (2, 1, 0, 5),
)

PLAN = ((END_PROGRAM, MID_PROGRAM), PIECES)


def plane_kernel(
    plan, tiles,
    own, middle, weights, gate_in, up_in, down_in, sgate_in, sup_in, sdown_in,
    out,
    rows_all, partial, from_level, from_side, table, scale,
    gate, up, down, sgate, sup, sdown, hidden, shared,
    load_sem, twin_send, twin_recv, w_send, w_recv,
    row_recv, level_recv, side_recv, send_sem,
):
    programs, pieces = plan
    experts = lax.axis_size("ep")
    me = lax.axis_index("ep")
    core = lax.rem(me, 2)
    node = me // 2
    col = lax.rem(node, 2)
    level = node // 2
    nodes = experts // 2
    top = nodes // 2 - 1
    rows, width = own.shape
    tile = rows // tiles
    hid = sgate.shape[1]
    flipped = level * 2 > top
    upward = jnp.where(flipped, -1, 1)
    twin = node * 2 + 1 - core

    def to_level(q):
        return jnp.where(flipped, top - q, q)

    def to_col(rel):
        return col if rel == 0 else 1 - col

    def to_node(q, rel):
        return to_level(q) * 2 + to_col(rel)

    def region(base, piece):
        at, high, left, wide = pieces[piece][1:]
        return (
            pl.ds(pl.multiple_of(base * rows + at * tile, tile), high * tile),
            pl.ds(left * width // 8, wide * width // 8),
        )

    loads = [
        pltpu.make_async_copy(src, dst, load_sem.at[n])
        for n, (src, dst) in enumerate(
            (
                (sgate_in, sgate), (sup_in, sup), (sdown_in, sdown),
                (gate_in.at[0], gate.at[core]), (up_in.at[0], up.at[core]),
                (down_in.at[0], down.at[pl.ds(pl.multiple_of(core * hid, hid), hid)]),
            )
        )
    ]
    for load in loads:
        load.start()

    barrier = pltpu.get_barrier_semaphore()
    for step in range(1, experts):
        pl.semaphore_signal(
            barrier, inc=1, device_id={"ep": lax.rem(me + step, experts)}, device_id_type=MESH
        )
    pl.semaphore_wait(barrier, experts - 1)

    def remote(src, dst, send, recv, target):
        return pltpu.make_async_remote_copy(
            src_ref=src, dst_ref=dst, send_sem=send, recv_sem=recv,
            device_id={"ep": target}, device_id_type=MESH,
        )

    always = []
    for step in range(1, nodes):
        other = lax.rem(node + step, nodes)
        copy = remote(
            weights.at[pl.ds(other * 2, 2)], table.at[node],
            w_send.at[step], w_recv.at[nodes - step], other * 2 + core,
        )
        copy.start()
        always.append(copy)
    twins = [
        remote(src, dst, twin_send.at[n], twin_recv.at[n], twin)
        for n, (src, dst) in enumerate(
            (
                (gate_in.at[0], gate.at[core]), (up_in.at[0], up.at[core]),
                (down_in.at[0], down.at[pl.ds(pl.multiple_of(core * hid, hid), hid)]),
            )
        )
    ]

    def twin_ready(n):
        refs = (gate.at[1 - core], up.at[1 - core],
                down.at[pl.ds(pl.multiple_of((1 - core) * hid, hid), hid)])
        remote(refs[n], refs[n], twin_send.at[n], twin_recv.at[n], twin).wait_recv()

    def strips(spot, first, others, store):
        row, lanes = spot
        wide = lanes.size
        step = 512 if wide % 512 == 0 else 256

        def strip(n, carry):
            at = pl.ds(pl.multiple_of(lanes.start + n * step, 128), step)
            value = first[row, at].astype(jnp.float32)
            for view in others:
                value = value + view(at).astype(jnp.float32)
            store(at, value)
            return carry

        lax.fori_loop(0, wide // step, strip, 0)

    def feed_in(base, source, take, gates, chunks, factor):
        def first(n, carry):
            data = source()
            gate_w, up_w = gates(n)
            g = jnp.dot(data, gate_w, preferred_element_type=jnp.float32)
            u = jnp.dot(data, up_w, preferred_element_type=jnp.float32)
            at = pl.ds(pl.multiple_of(n * 256, 256), 256)
            hidden[pl.ds(base, take), at] = factor(n, jax.nn.silu(g) * u).astype(jnp.bfloat16)
            return carry

        lax.fori_loop(0, chunks, first, 0)

    def feed_out(base, take, depth, down_w, finish):
        def second(n, carry):
            cols = pl.ds(pl.multiple_of(n * 512, 512), 512)
            piece = jnp.dot(
                hidden[pl.ds(base, take), pl.ds(0, depth)], down_w[:, cols],
                preferred_element_type=jnp.float32,
            )
            finish(cols, piece.astype(jnp.bfloat16))
            return carry

        lax.fori_loop(0, width // 512, second, 0)

    halves = hid // 256
    depths = hidden.shape[0] // (4 * rows)

    def shared_expert():
        for load in loads[:3]:
            load.wait()

        def gates(n):
            cols = pl.ds(pl.multiple_of(n * 256, 256), 256)
            return sgate[:, cols], sup[:, cols]

        feed_in(0, lambda: own[...], rows, gates, halves, lambda n, value: value)

        def keep(cols, piece):
            shared[:, cols] = piece

        feed_out(0, rows, hid, sdown, keep)

    def spread_table():
        for step in range(1, nodes):
            other = lax.rem(node + step, nodes)
            remote(
                table.at[other], table.at[other], w_send.at[step], w_recv.at[step], twin
            ).wait_recv()
        table[node] = weights[pl.ds(node * 2, 2)]

        def one(n, carry):
            for e in range(2):
                line = jnp.broadcast_to(table[n, e], (128, 128))
                scale[e, pl.ds(pl.multiple_of(n * rows, tile), rows), :] = jnp.transpose(line)[:rows]
            return carry

        lax.fori_loop(0, nodes, one, 0)

    def run(program, position):
        sends = []
        landed = set()
        dealt = set()
        held = {}

        def push(src, dst, recv, target):
            copy = remote(src, dst, send_sem.at[len(sends)], recv, target)
            copy.start()
            sends.append(copy)

        def row_in(q, rel, piece):
            if (q, rel) == (position, 0) or (q, rel, piece) in landed:
                return
            landed.add((q, rel, piece))
            origin = to_node(q, rel)
            view = rows_all.at[region(origin, piece)]
            remote(view, view, send_sem.at[0], row_recv.at[origin, piece], twin).wait_recv()

        def neighbour(way):
            if way == 2:
                return level * 2 + 1 - col
            return (level + (upward if way == 0 else -upward)) * 2 + col

        def pass_row(q, rel, piece, way):
            row_in(q, rel, piece)
            origin = to_node(q, rel)
            if (q, rel) == (position, 0):
                src = own.at[region(0, piece)]
            else:
                src = rows_all.at[region(origin, piece)]
            push(
                src, rows_all.at[region(origin, piece)], row_recv.at[origin, piece],
                neighbour(way) * 2 + core,
            )

        def level_slot(goal, same, below):
            if not same:
                return goal
            return jnp.where(below, goal, nodes + lax.rem(goal, 2))

        def gathered(q, rel, piece):
            across = pieces[piece][0] == 0
            views = []
            goal = to_node(q, rel)
            waits = []
            if across and rel == 1:
                return views
            if (q == position and rel == 0) or (across and rel == 0):
                spot = to_level(q)
                waits.append((from_side, spot, side_recv))
            if q >= position and position > 0:
                slot = level_slot(goal, q == position, jnp.logical_not(flipped))
                waits.append((from_level, slot, level_recv))
            if q <= position:
                slot = level_slot(goal, q == position, flipped)
                waits.append((from_level, slot, level_recv))
            for ref, slot, recv in waits:
                view = ref.at[region(slot, piece)]
                remote(view, view, send_sem.at[0], recv.at[slot, piece], twin).wait_recv()
                row = region(slot, piece)[0]
                views.append(lambda at, ref=ref, row=row: ref[row, at])
            return views

        def collect(q, rel, piece):
            if (q, rel, piece) in dealt:
                return
            dealt.add((q, rel, piece))
            views = gathered(q, rel, piece)
            if not views:
                return
            spot = region(to_node(q, rel), piece)

            def store(at, value):
                partial[spot[0], at] = value.astype(jnp.bfloat16)

            strips(spot, partial, views, store)

        def pass_sum(q, rel, piece, way):
            collect(q, rel, piece)
            goal = to_node(q, rel)
            spot = region(goal, piece)
            if way == 2:
                slot = to_level(q)
                dst, recv = from_side.at[region(slot, piece)], side_recv.at[slot, piece]
            else:
                beside = position + (1 if way == 0 else -1)
                below = jnp.logical_not(flipped) if way == 0 else flipped
                slot = level_slot(goal, beside == q, below)
                dst, recv = from_level.at[region(slot, piece)], level_recv.at[slot, piece]
            push(partial.at[spot], dst, recv, neighbour(way) * 2 + core)

        def finish(q, rel, piece):
            views = gathered(q, rel, piece)
            spot = region(to_node(q, rel), piece)
            local = region(0, piece)[0]
            views = views + [lambda at: shared[local, at], lambda at: middle[local, at]]

            def store(at, value):
                out[local, at] = value.astype(jnp.bfloat16)

            strips(spot, partial, views, store)

        def slices(block):
            found = []
            for q, groups in block:
                for rel in (0, 1):
                    base = to_node(q, rel) * rows
                    runs = []
                    for g in groups:
                        if runs and runs[-1][1] == g:
                            runs[-1][1] = g + 1
                        else:
                            runs.append([g, g + 1])
                    for begin, end in runs:
                        size = (end - begin) * 2 * tile
                        at = pl.multiple_of(base + begin * 2 * tile, tile)
                        found.append((pl.ds(at, size), size))
            return found

        def block_in(block):
            for q, groups in block:
                for rel in (0, 1):
                    for piece, spec in enumerate(pieces):
                        if spec[1] // 2 in groups:
                            row_in(q, rel, piece)
            spots = slices(block)
            take = sum(size for _, size in spots)

            def source():
                return jnp.concatenate([rows_all[at, :] for at, _ in spots], axis=0)

            def gates(n):
                cols = pl.ds(pl.multiple_of(lax.rem(n, halves) * 256, 256), 256)
                return gate[n // halves, :, cols], up[n // halves, :, cols]

            def factor(n, value):
                lines = jnp.concatenate([scale[n // halves, at, :] for at, _ in spots], axis=0)
                return value * jnp.concatenate([lines, lines], axis=1)

            held[block] = min(set(range(depths)) - set(held.values()))
            feed_in(held[block] * 4 * rows, source, take, gates, 2 * halves, factor)

        def block_out(block):
            spots = slices(block)
            take = sum(size for _, size in spots)

            def keep(cols, piece):
                at = 0
                for spot, size in spots:
                    partial[spot, cols] = piece[at:at + size]
                    at += size

            feed_out(held.pop(block) * 4 * rows, take, 2 * hid, down, keep)

        begun = False
        ended = False
        for act in program:
            kind = act[0]
            if kind == 0:
                pass_row(*act[1:])
            elif kind == 1:
                pass_sum(*act[1:])
            elif kind == 2:
                finish(*act[1:])
            elif kind == 3:
                if not begun:
                    begun = True
                    spread_table()
                    for load in loads[3:5]:
                        load.wait()
                    twin_ready(0)
                    twin_ready(1)
                block_in(act[1])
            elif kind == 4:
                if not ended:
                    ended = True
                    loads[5].wait()
                    twin_ready(2)
                block_out(act[1])
            elif kind == 5:
                for copy in twins:
                    copy.start()
                rows_all[pl.ds(pl.multiple_of(node * rows, tile), rows), :] = own[...]
                shared_expert()
        for copy in sends:
            copy.wait_send()


    for position, program in enumerate(programs):
        near_end = jnp.logical_or(level == position, level == top - position)
        pl.when(near_end)(functools.partial(run, program, position))
    for copy in always + twins:
        copy.wait_send()


def plane_stage(
    second_normed, middle, routes, route_weights,
    expert_gate, expert_up, expert_down, shared_gate, shared_up, shared_down,
):
    experts = lax.axis_size("ep")
    nodes = experts // 2
    rows, width = second_normed.shape
    hid = expert_gate.shape[2]
    tiles = 6
    chosen = routes[None, :, :] == jnp.arange(experts, dtype=jnp.int32)[:, None, None]
    weights = jnp.sum(jnp.where(chosen, route_weights[None], 0.0), axis=2)
    weights = jnp.pad(weights, ((0, 0), (0, 128 - rows)))[:, None, :]
    vmem = pl.BlockSpec(memory_space=pltpu.VMEM)
    hbm = pl.BlockSpec(memory_space=pl.ANY)
    dma = pltpu.SemaphoreType.DMA
    half = jnp.bfloat16
    programs, pieces = PLAN
    count = len(pieces)
    most = max(sum(act[0] < 2 for act in program) for program in programs)
    return pl.pallas_call(
        functools.partial(plane_kernel, PLAN, tiles),
        out_shape=jax.ShapeDtypeStruct((rows, width), half),
        in_specs=[vmem] * 3 + [hbm] * 6,
        out_specs=vmem,
        scratch_shapes=[
            pltpu.VMEM((nodes * rows, width), half),
            pltpu.VMEM((nodes * rows, width), half),
            pltpu.VMEM(((nodes + 2) * rows, width), half),
            pltpu.VMEM((nodes // 2 * rows, width), half),
            pltpu.VMEM((nodes, 2, 1, 128), jnp.float32),
            pltpu.VMEM((2, nodes * rows, 128), jnp.float32),
            pltpu.VMEM((2, width, hid), half),
            pltpu.VMEM((2, width, hid), half),
            pltpu.VMEM((2 * hid, width), half),
            pltpu.VMEM(shared_gate.shape, half),
            pltpu.VMEM(shared_up.shape, half),
            pltpu.VMEM(shared_down.shape, half),
            pltpu.VMEM((3 * 4 * rows, 2 * hid), half),
            pltpu.VMEM((rows, width), half),
            dma((6,)),
            dma((3,)),
            dma((3,)),
            dma((nodes,)),
            dma((nodes,)),
            dma((nodes, count)),
            dma((nodes + 2, count)),
            dma((nodes // 2, count)),
            dma((most,)),
        ],
        compiler_params=pltpu.CompilerParams(
            collective_id=0, has_side_effects=True, vmem_limit_bytes=60 * 1024 * 1024
        ),
    )(
        second_normed, middle, weights,
        expert_gate, expert_up, expert_down, shared_gate, shared_up, shared_down,
    )


def mixer_kernel(
    tokens, prior, mix_gain, in_weight, params, input_map, output_map, skip, out_weight,
    channel_gain, new_state, middle, second, normed, acts, acc,
):
    step = pl.program_id(0)
    lane = 128
    channels = in_weight.shape[1]
    width = input_map.shape[2]
    group = acts.shape[1] * width // prior.shape[2]
    per = lane // group
    states = per * width

    def scaled(values, gain):
        factor = lax.rsqrt(jnp.mean(values * values, axis=-1, keepdims=True) + norm_eps)
        return (values * factor * gain[...]).astype(jnp.bfloat16)

    @pl.when(step == 0)
    def _():
        normed[...] = scaled(tokens[...].astype(jnp.float32), mix_gain)
        acc[...] = jnp.zeros_like(acc)

    drive = jnp.dot(normed[...], in_weight[...], preferred_element_type=jnp.float32)
    drive = drive.astype(jnp.bfloat16)
    row = lax.broadcasted_iota(jnp.int32, (lane, states), 0) // group
    column = lax.broadcasted_iota(jnp.int32, (lane, states), 1) // width
    own_group = row == column

    def spread(table):
        tiled = jnp.concatenate([table] * per, axis=1)
        return jnp.where(own_group, tiled, 0.0).astype(jnp.bfloat16)

    for sub in range(channels // lane):
        cols = slice(sub * lane, (sub + 1) * lane)
        ent = slice(sub * states, (sub + 1) * states)
        part = drive[:, cols]
        push_real = jnp.dot(
            part, spread(input_map[0, cols, :]), preferred_element_type=jnp.float32
        )
        push_imag = jnp.dot(
            part, spread(input_map[1, cols, :]), preferred_element_type=jnp.float32
        )
        turn_real, turn_imag = params[0:1, ent], params[1:2, ent]
        hold_real, hold_imag = params[2:3, ent], params[3:4, ent]
        old_real, old_imag = prior[0, :, ent], prior[1, :, ent]
        fresh_real = (
            turn_real * old_real - turn_imag * old_imag
            + (push_real * hold_real - push_imag * hold_imag)
        )
        fresh_imag = (
            turn_real * old_imag + turn_imag * old_real
            + (push_real * hold_imag + push_imag * hold_real)
        )
        new_state[0, :, ent] = fresh_real
        new_state[1, :, ent] = fresh_imag
        across = (((1,), (1,)), ((), ()))
        readout = lax.dot_general(
            fresh_real.astype(jnp.bfloat16), spread(output_map[0, cols, :]), across,
            preferred_element_type=jnp.float32,
        ) - lax.dot_general(
            fresh_imag.astype(jnp.bfloat16), spread(output_map[1, cols, :]), across,
            preferred_element_type=jnp.float32,
        )
        readout = readout + skip[:, cols] * part.astype(jnp.float32)
        acts[:, cols] = jax.nn.gelu(readout).astype(jnp.bfloat16)
    acc[...] += jnp.dot(acts[...], out_weight[...], preferred_element_type=jnp.float32)

    @pl.when(step == pl.num_programs(0) - 1)
    def _():
        mixed = acc[...].astype(jnp.bfloat16).astype(jnp.float32)
        mid = (tokens[...].astype(jnp.float32) + mixed).astype(jnp.bfloat16)
        middle[...] = mid
        second[...] = scaled(mid.astype(jnp.float32), channel_gain)


def mixer_stage(
    tokens, prior_state, mix_gain, in_weight, decay_rate, frequency, log_step,
    input_map, output_map, skip_gain, out_weight, channel_gain,
):
    rows, model = tokens.shape
    groups, width = decay_rate.shape
    channels = in_weight.shape[1]
    step_size = jnp.exp(log_step)[:, None]
    real_rate = -decay_rate
    magnitude = jnp.exp(real_rate * step_size)
    turn_real = magnitude * jnp.cos(frequency * step_size)
    turn_imag = magnitude * jnp.sin(frequency * step_size)
    denominator = real_rate * real_rate + frequency * frequency
    hold_real = ((turn_real - 1.0) * real_rate + turn_imag * frequency) / denominator
    hold_imag = (turn_imag * real_rate - (turn_real - 1.0) * frequency) / denominator
    params = jnp.stack([turn_real, turn_imag, hold_real, hold_imag]).reshape(4, -1)
    in_map = jnp.transpose(input_map, (0, 1, 3, 2)).reshape(2, channels, width)
    out_map = output_map.reshape(2, channels, width)
    block = 256
    states = block * groups * width // channels

    def whole(*shape):
        return pl.BlockSpec(shape, lambda i: (0,) * len(shape))

    half = jnp.bfloat16
    return pl.pallas_call(
        mixer_kernel,
        grid=(channels // block,),
        out_shape=(
            jax.ShapeDtypeStruct(prior_state.shape, jnp.float32),
            jax.ShapeDtypeStruct((rows, model), half),
            jax.ShapeDtypeStruct((rows, model), half),
        ),
        in_specs=[
            whole(rows, model),
            pl.BlockSpec((2, rows, states), lambda i: (0, 0, i)),
            whole(1, model),
            pl.BlockSpec((model, block), lambda i: (0, i)),
            pl.BlockSpec((4, states), lambda i: (0, i)),
            pl.BlockSpec((2, block, width), lambda i: (0, i, 0)),
            pl.BlockSpec((2, block, width), lambda i: (0, i, 0)),
            pl.BlockSpec((1, block), lambda i: (0, i)),
            pl.BlockSpec((block, model), lambda i: (i, 0)),
            whole(1, model),
        ],
        out_specs=(
            pl.BlockSpec((2, rows, states), lambda i: (0, 0, i)),
            whole(rows, model),
            whole(rows, model),
        ),
        scratch_shapes=[
            pltpu.VMEM((rows, model), half),
            pltpu.VMEM((rows, block), half),
            pltpu.VMEM((rows, model), jnp.float32),
        ],
        compiler_params=pltpu.CompilerParams(
            dimension_semantics=("arbitrary",), vmem_limit_bytes=62 * 1024 * 1024
        ),
    )(
        tokens, prior_state, mix_gain[None], in_weight, params, in_map, out_map,
        skip_gain[None], out_weight, channel_gain[None],
    )


def body(
    tokens,
    prior_state,
    mix_gain,
    in_weight,
    decay_rate,
    frequency,
    log_step,
    input_map,
    output_map,
    skip_gain,
    out_weight,
    channel_gain,
    expert_gate,
    expert_up,
    expert_down,
    shared_gate,
    shared_up,
    shared_down,
    routes,
    route_weights,
):
    if lax.axis_size("tp") == 1 and lax.axis_size("ep") == 16:
        new_state, middle, second_normed = mixer_stage(
            tokens, prior_state, mix_gain, in_weight, decay_rate, frequency, log_step,
            input_map, output_map, skip_gain, out_weight, channel_gain,
        )
        layer_out = plane_stage(
            second_normed, middle, routes, route_weights,
            expert_gate, expert_up, expert_down, shared_gate, shared_up, shared_down,
        )
        return (layer_out, new_state)
    normed = root_scale(tokens, mix_gain)
    drive_rows = jnp.dot(normed, in_weight, preferred_element_type=jnp.float32).astype(jnp.bfloat16)
    readout, new_state = state_update(
        drive_rows, prior_state, decay_rate, frequency, log_step, input_map, output_map, skip_gain
    )
    activated = jax.nn.gelu(readout).astype(jnp.bfloat16)
    partial_value = jnp.dot(activated, out_weight, preferred_element_type=jnp.float32)
    mixer_out = lax.psum(partial_value.astype(jnp.bfloat16), "tp").astype(jnp.float32)
    middle = (tokens.astype(jnp.float32) + mixer_out).astype(jnp.bfloat16)
    second_normed = root_scale(middle, channel_gain)
    shared_gval = jnp.dot(second_normed, shared_gate, preferred_element_type=jnp.float32)
    shared_uval = jnp.dot(second_normed, shared_up, preferred_element_type=jnp.float32)
    shared_hidden = (jax.nn.silu(shared_gval) * shared_uval).astype(jnp.bfloat16)
    shared_piece = jnp.dot(shared_hidden, shared_down, preferred_element_type=jnp.float32)
    shared_out = lax.psum_scatter(
        shared_piece.astype(jnp.bfloat16), "tp", scatter_dimension=1, tiled=True
    ).astype(jnp.float32)
    half_cols = second_normed.shape[1] // lax.axis_size("tp")
    routed = exchanged_experts(
        second_normed, routes, route_weights, expert_gate, expert_up, expert_down
    )
    own_middle = lax.dynamic_slice_in_dim(middle, lax.axis_index("tp") * half_cols, half_cols, 1)
    layer_out = (own_middle.astype(jnp.float32) + routed + shared_out).astype(jnp.bfloat16)
    return (layer_out, new_state)


def solution(mesh):
    in_specs = (
        P(("grp", "ep"), None),
        P(None, ("grp", "ep"), "tp"),
        P(),
        P(None, "tp"),
        P("tp", None),
        P("tp", None),
        P("tp"),
        P(None, "tp", None, None),
        P(None, "tp", None, None),
        P("tp"),
        P("tp", None),
        P(),
        P("ep", None, "tp"),
        P("ep", None, "tp"),
        P("ep", "tp", None),
        P(None, "tp"),
        P(None, "tp"),
        P("tp", None),
        P(("grp", "ep"), None),
        P(("grp", "ep"), None),
    )
    out_specs = (P(("grp", "ep"), "tp"), P(None, ("grp", "ep"), "tp"))
    return jax.shard_map(body, mesh=mesh, in_specs=in_specs, out_specs=out_specs, check_vma=False)
```

time: 102 us -> 84.2 us (0.83)
  Pallas kernels: 95.5 us -> 77.5 us
    pallas_call x1, Pallas kernels: 85.1 us -> 67.1 us  [plane_stage(): pl.pallas_call(functools.partial(plane_kernel, PLAN, tiles), out_shape=ja...]
where the time goes in v1:
time: 84.2 us; the launch traced here: 83.9 us
  Pallas kernels  77.5 us (92%)
  local copies, waits for them, and re-layouts  3.36 us (4%)
  other arithmetic  2.4 us (3%)
    pallas_call x1, Pallas kernels, plane_stage(): pl.pallas_call(functools.partial(plane_kernel, PLAN, tiles), out_shape=ja...  67.1 us
    pallas_call x1, Pallas kernels, mixer_stage(): pl.pallas_call(mixer_kernel, grid=(channels // block,), out_shape=(jax.Sh...  10.4 us
    unnamed x1, local copies, waits for them, and re-layouts  1.77 us

profile of v1, /device:TPU:0, one launch (start us, length us, event | category | flops | bytes accessed | tf_op | source)
XLA Modules:
  0.0 83.9 jit_solution(3059535620123851418)
XLA Ops:
  0.6 0.7 exp.6
  1.3 0.7 select_reduce_fusion
  2.0 0.6 pad.4
  2.6 1.0 %cosine_multiply_fusion = (f32[64,64]{1,0:T(8,128)S(1)}, f32[64,64]{1,0:T(8,128)S(1)}, f32[64,64]{1,0:T(8,128)S(1)}, f32[64,64]{1,0:T(8,128)S(1)}) fusion(f32[64,64]{1,0:T(8,128)} %param.25, f32[64,64]{1,0:T(8,128)} %param.24, f32[64]{0:T(128)S(1)} %exp.6), kind=kLoop, calls=%fused_computation.7 | loop fusion | flops 69632 | bytes 98560 | tf_op jit(solution)/shard_map/mul | solution.py:660
  3.6 0.1 stack.15
  3.7 0.1 stack.17
  3.8 0.1 stack.18
  3.9 0.1 stack.16
  4.0 0.7 pad_maximum_fusion.params
  4.7 10.4 %shard_map.203 = (f32[2,96,4096]{2,1,0:T(8,128)}, bf16[96,2048]{1,0:T(8,128)(2,1)}, bf16[96,2048]{1,0:T(8,128)(2,1)}) custom-call(bf16[96,2048]{1,0:T(8,128)(2,1)} %tokens.1, f32[2,96,4096]{2,1,0:T(8,128)} %prior.1, f32[1,2048]{1,0:T(1,128)} %bitcast.11, bf16[2048,1024]{1,0:T(8,128)(2,1)} %in_weight.1, f32[4,4096]{1,0:T(4,128)} %pad_maximum_fusion.params, ...), custom_call_target="tpu_custom_call" | custom-call | tf_op jit(solution)/shard_map/pallas_call | solution.py:675
  15.0 67.1 %shard_map.204 = bf16[96,2048]{1,0:T(8,128)(2,1)} custom-call(bf16[96,2048]{1,0:T(8,128)(2,1)} %get-tuple-element.5.own, bf16[96,2048]{1,0:T(8,128)(2,1)} %get-tuple-element.6.middle, f32[16,1,128]{2,1,0:T(1,128)} %bitcast.10, bf16[1,2048,512]{2,1,0:T(8,128)(2,1)} %gate_in.1, bf16[1,2048,512]{2,1,0:T(8,128)(2,1)} %up_in.1, bf16[1,512,2048]{2,1,0:T(8,128)(2,1)} %down_in.1, ...), custom_call_target="tpu_custom_call" | custom-call | tf_op jit(solution)/shard_map/pallas_call | solution.py:537
  82.1 1.8 %copy.25 = bf16[96,2048]{1,0:T(8,128)(2,1)} copy(bf16[96,2048]{1,0:T(8,128)(2,1)} %shard_map.204) | data formatting | bytes 786432

commit v2 on v1

--- a/solution.py
+++ b/solution.py
@@ -92,32 +92,32 @@
     (1, 2, 1, 0, 8),
     (0, 3, 1, 0, 8),
     (0, 4, 1, 0, 8),
-    (0, 5, 1, 0, 5),
-    (1, 5, 1, 5, 3),
+    (0, 5, 1, 0, 4),
+    (1, 5, 1, 4, 4),
 )
 
 END_PROGRAM = (
     (0, 0, 0, 0, 2), (0, 0, 0, 0, 0), (0, 0, 0, 1, 2), (0, 0, 0, 1, 0), (0, 0, 0, 3, 2),
     (0, 0, 0, 2, 2), (0, 0, 0, 3, 0), (5,), (0, 0, 1, 0, 0), (0, 0, 0, 2, 0), (0, 0, 0, 4, 0),
     (0, 1, 0, 1, 2), (0, 1, 0, 3, 2), (0, 0, 0, 4, 2), (0, 0, 1, 2, 0), (0, 0, 0, 5, 0),
-    (0, 0, 0, 6, 0), (3, ((0, (0,)),)), (0, 2, 0, 1, 2), (0, 0, 0, 5, 2), (0, 0, 0, 6, 2),
-    (3, ((1, (0,)),)), (4, ((0, (0,)),)), (1, 0, 1, 1, 2), (4, ((1, (0,)),)), (1, 1, 0, 0, 0),
-    (1, 1, 1, 0, 0), (0, 3, 0, 1, 2), (1, 1, 1, 1, 2), (0, 0, 1, 6, 0), (3, ((2, (0,)),)),
-    (4, ((2, (0,)),)), (1, 2, 0, 0, 0), (1, 2, 1, 0, 0), (1, 2, 1, 1, 2), (0, 3, 0, 3, 2),
-    (3, ((3, (0,)),)), (0, 2, 0, 3, 2), (4, ((3, (0,)),)), (1, 3, 0, 0, 0), (1, 3, 1, 0, 0),
-    (1, 3, 1, 1, 2), (1, 2, 0, 1, 0), (1, 1, 0, 1, 0), (3, ((2, (1,)), (3, (1,)))),
-    (1, 3, 0, 1, 0), (4, ((2, (1,)), (3, (1,)))), (0, 3, 0, 4, 2), (1, 3, 0, 2, 0),
-    (1, 3, 1, 2, 0), (1, 3, 1, 3, 2), (1, 2, 0, 2, 0), (1, 2, 1, 2, 0), (1, 2, 1, 3, 2),
-    (0, 3, 0, 5, 2), (3, ((1, (1,)),)), (4, ((1, (1,)),)), (0, 2, 0, 4, 2), (1, 3, 0, 3, 0),
-    (1, 1, 1, 3, 2), (0, 2, 0, 5, 2), (1, 2, 0, 3, 0), (1, 1, 0, 2, 0), (1, 1, 1, 2, 0),
-    (0, 1, 0, 4, 2), (0, 1, 0, 5, 2), (3, ((0, (1,)), (3, (2,)))), (4, ((0, (1,)), (3, (2,)))),
-    (1, 3, 0, 6, 0), (1, 3, 1, 4, 2), (1, 3, 1, 5, 2), (1, 3, 1, 6, 0), (1, 1, 0, 3, 0),
-    (3, ((2, (2,)),)), (4, ((2, (2,)),)), (1, 2, 0, 6, 0), (1, 2, 1, 4, 2), (1, 2, 1, 5, 2),
-    (1, 0, 1, 0, 2), (3, ((0, (2,)), (1, (2,)))), (1, 3, 0, 4, 0), (4, ((0, (2,)), (1, (2,)))),
-    (1, 3, 0, 5, 0), (1, 2, 1, 6, 0), (1, 1, 1, 4, 2), (1, 1, 1, 5, 2), (2, 0, 0, 1),
-    (1, 2, 0, 4, 0), (1, 2, 0, 5, 0), (1, 1, 0, 6, 0), (1, 1, 1, 6, 0), (1, 0, 1, 2, 2),
-    (1, 0, 1, 3, 2), (2, 0, 0, 0), (1, 1, 0, 4, 0), (1, 1, 0, 5, 0), (1, 0, 1, 6, 2),
-    (1, 0, 1, 4, 2), (1, 0, 1, 5, 2), (2, 0, 0, 2), (2, 0, 0, 3), (2, 0, 0, 6), (2, 0, 0, 4),
+    (0, 0, 0, 6, 0), (0, 2, 0, 1, 2), (0, 0, 0, 5, 2), (0, 0, 0, 6, 2),
+    (3, ((0, (1,)), (1, (0,)))), (4, ((0, (1,)), (1, (0,)))), (1, 1, 0, 0, 0), (1, 1, 1, 0, 0),
+    (1, 1, 1, 1, 2), (0, 3, 0, 1, 2), (1, 0, 1, 3, 2), (0, 0, 1, 6, 0), (3, ((2, (0,)),)),
+    (4, ((2, (0,)),)), (1, 2, 0, 0, 0), (1, 2, 1, 0, 0), (1, 2, 1, 1, 2), (1, 1, 0, 1, 0),
+    (0, 3, 0, 3, 2), (3, ((3, (0,)),)), (0, 2, 0, 3, 2), (4, ((3, (0,)),)), (1, 3, 0, 0, 0),
+    (1, 3, 1, 0, 0), (1, 3, 1, 1, 2), (1, 2, 0, 1, 0), (3, ((0, (0,)), (3, (1,)))),
+    (4, ((0, (0,)), (3, (1,)))), (1, 3, 0, 2, 0), (1, 3, 1, 2, 0), (1, 3, 1, 3, 2),
+    (1, 0, 1, 1, 2), (3, ((2, (1,)),)), (1, 3, 0, 1, 0), (4, ((2, (1,)),)), (1, 2, 0, 2, 0),
+    (1, 2, 1, 2, 0), (1, 2, 1, 3, 2), (0, 3, 0, 4, 2), (0, 3, 0, 5, 2), (1, 3, 0, 3, 0),
+    (3, ((1, (1,)),)), (0, 2, 0, 4, 2), (4, ((1, (1,)),)), (1, 2, 0, 3, 0), (1, 1, 0, 2, 0),
+    (1, 1, 1, 3, 2), (0, 2, 0, 5, 2), (3, ((3, (2,)),)), (0, 1, 0, 4, 2), (4, ((3, (2,)),)),
+    (1, 3, 0, 6, 0), (1, 3, 1, 4, 2), (1, 3, 1, 5, 2), (0, 1, 0, 5, 2), (1, 3, 1, 6, 0),
+    (1, 1, 1, 2, 0), (3, ((2, (2,)),)), (4, ((2, (2,)),)), (1, 2, 0, 6, 0), (1, 2, 1, 4, 2),
+    (1, 2, 1, 5, 2), (1, 2, 1, 6, 0), (1, 3, 0, 4, 0), (1, 0, 1, 2, 2), (1, 3, 0, 5, 0),
+    (1, 1, 0, 3, 0), (3, ((0, (2,)), (1, (2,)))), (4, ((0, (2,)), (1, (2,)))), (1, 2, 0, 4, 0),
+    (1, 1, 0, 6, 0), (1, 1, 1, 4, 2), (1, 1, 1, 6, 0), (1, 0, 1, 0, 2), (1, 1, 1, 5, 2),
+    (1, 0, 1, 4, 2), (1, 2, 0, 5, 0), (2, 0, 0, 2), (2, 0, 0, 1), (2, 0, 0, 0), (1, 0, 1, 6, 2),
+    (1, 0, 1, 5, 2), (1, 1, 0, 4, 0), (1, 1, 0, 5, 0), (2, 0, 0, 3), (2, 0, 0, 6), (2, 0, 0, 4),
     (2, 0, 0, 5),
 )
 
@@ -126,30 +126,31 @@
     (0, 1, 0, 1, 1), (0, 1, 0, 3, 2), (0, 1, 0, 2, 2), (0, 1, 0, 3, 0), (0, 1, 0, 3, 1), (5,),
     (0, 0, 0, 0, 0), (0, 2, 0, 0, 1), (0, 0, 0, 1, 2), (0, 0, 0, 1, 0), (0, 1, 1, 0, 0),
     (0, 2, 0, 1, 2), (0, 2, 0, 1, 1), (0, 1, 1, 0, 1), (0, 0, 0, 3, 2), (0, 0, 1, 0, 0),
-    (0, 0, 0, 3, 0), (0, 3, 0, 0, 1), (3, ((1, (0,)),)), (0, 0, 0, 2, 0), (0, 3, 0, 1, 2),
-    (0, 2, 0, 3, 2), (0, 3, 0, 1, 1), (0, 2, 1, 0, 1), (4, ((1, (0,)),)), (1, 1, 1, 1, 2),
-    (0, 0, 1, 2, 0), (0, 1, 0, 2, 0), (0, 1, 1, 2, 0), (0, 0, 0, 4, 0), (0, 3, 1, 0, 1),
-    (0, 0, 0, 5, 0), (0, 1, 0, 4, 0), (0, 1, 0, 5, 0), (0, 0, 0, 6, 0), (0, 3, 0, 3, 2),
-    (0, 0, 0, 4, 2), (0, 0, 0, 5, 2), (0, 1, 0, 4, 2), (0, 1, 0, 5, 2), (0, 1, 0, 6, 2),
-    (0, 3, 0, 3, 1), (0, 2, 0, 3, 1), (0, 3, 0, 2, 1), (0, 3, 1, 2, 1), (0, 2, 0, 2, 1),
-    (0, 2, 1, 2, 1), (0, 0, 1, 6, 0), (0, 1, 0, 6, 0), (0, 3, 0, 4, 2), (0, 3, 0, 4, 1),
-    (0, 3, 0, 5, 2), (0, 3, 0, 5, 1), (0, 1, 0, 2, 1), (0, 1, 1, 2, 1), (0, 2, 0, 4, 2),
-    (0, 2, 0, 4, 1), (0, 1, 1, 6, 0), (3, ((0, (1,)), (1, (1, 2)), (2, (0,)))), (0, 2, 0, 5, 2),
-    (0, 2, 0, 5, 1), (0, 1, 0, 4, 1), (0, 1, 0, 5, 1), (0, 3, 0, 6, 1), (0, 3, 1, 6, 1),
-    (0, 2, 0, 6, 1), (4, ((0, (1,)), (1, (1, 2)), (2, (0,)))), (0, 2, 1, 6, 1), (1, 0, 1, 3, 2),
-    (1, 2, 0, 0, 0), (1, 2, 1, 0, 0), (1, 2, 1, 1, 2), (1, 1, 1, 3, 2),
-    (3, ((0, (0,)), (3, (0, 2)))), (4, ((0, (0,)), (3, (0, 2)))), (1, 3, 0, 0, 0),
-    (1, 3, 1, 0, 0), (1, 3, 1, 1, 2), (1, 3, 1, 4, 2), (3, ((0, (2,)), (2, (1, 2)), (3, (1,)))),
-    (1, 2, 0, 1, 0), (4, ((0, (2,)), (2, (1, 2)), (3, (1,)))), (1, 3, 0, 2, 0), (1, 3, 1, 3, 2),
-    (1, 3, 1, 5, 2), (1, 0, 1, 1, 2), (1, 0, 0, 0, 1), (1, 2, 1, 3, 2), (1, 1, 1, 0, 2),
-    (1, 2, 1, 4, 2), (1, 2, 1, 5, 2), (1, 0, 1, 4, 2), (1, 0, 1, 5, 2), (1, 3, 0, 1, 0),
-    (1, 3, 1, 2, 0), (1, 0, 1, 0, 1), (0, 1, 0, 6, 1), (0, 1, 1, 6, 1), (2, 1, 0, 1),
-    (1, 3, 0, 3, 0), (1, 2, 0, 2, 0), (1, 2, 1, 2, 0), (1, 0, 0, 2, 1), (1, 0, 0, 1, 1),
-    (1, 0, 1, 2, 1), (1, 3, 0, 6, 0), (1, 0, 0, 3, 1), (1, 3, 1, 6, 0), (1, 2, 0, 3, 0),
-    (2, 1, 0, 0), (1, 2, 0, 6, 0), (1, 1, 1, 2, 2), (1, 1, 1, 4, 2), (1, 1, 1, 5, 2),
-    (1, 0, 0, 6, 1), (1, 3, 0, 4, 0), (1, 0, 1, 6, 1), (1, 3, 0, 5, 0), (1, 2, 1, 6, 0),
-    (2, 1, 0, 3), (1, 2, 0, 4, 0), (2, 1, 0, 2), (1, 2, 0, 5, 0), (1, 0, 0, 4, 1),
-    (1, 0, 0, 5, 1), (1, 1, 1, 6, 2), (2, 1, 0, 4), (2, 1, 0, 6), (2, 1, 0, 5),
+    (0, 0, 0, 3, 0), (0, 3, 0, 0, 1), (0, 0, 0, 2, 0), (0, 3, 0, 1, 2), (0, 2, 0, 3, 2),
+    (0, 3, 0, 1, 1), (0, 0, 0, 4, 2), (0, 2, 1, 0, 1), (0, 0, 1, 2, 0), (0, 1, 0, 2, 0),
+    (0, 1, 1, 2, 0), (0, 0, 0, 4, 0), (0, 3, 1, 0, 1), (0, 0, 0, 5, 0), (0, 1, 0, 4, 0),
+    (0, 1, 0, 5, 0), (0, 3, 0, 3, 2), (0, 0, 0, 5, 2), (0, 1, 0, 4, 2), (0, 1, 0, 5, 2),
+    (0, 1, 0, 6, 2), (0, 3, 0, 3, 1), (0, 2, 0, 3, 1), (0, 0, 0, 6, 0), (0, 3, 0, 2, 1),
+    (0, 3, 1, 2, 1), (0, 2, 0, 2, 1), (0, 0, 1, 6, 0), (0, 1, 0, 6, 0),
+    (3, ((0, (2,)), (3, (1,)))), (0, 2, 1, 2, 1), (4, ((0, (2,)), (3, (1,)))), (0, 3, 0, 4, 2),
+    (0, 3, 0, 4, 1), (1, 3, 1, 3, 2), (1, 0, 1, 4, 2), (1, 0, 1, 5, 2), (0, 1, 1, 6, 0),
+    (0, 3, 0, 5, 1), (0, 1, 0, 2, 1), (0, 1, 1, 2, 1), (3, ((1, (1, 2)), (2, (0,)), (3, (0,)))),
+    (0, 2, 0, 4, 1), (0, 2, 0, 5, 1), (4, ((1, (1, 2)), (2, (0,)), (3, (0,)))), (0, 3, 0, 6, 1),
+    (0, 3, 1, 6, 1), (0, 1, 0, 4, 1), (0, 1, 0, 5, 1), (1, 3, 1, 1, 2), (1, 2, 0, 0, 0),
+    (1, 2, 1, 1, 2), (0, 3, 0, 5, 2), (1, 1, 1, 3, 2), (0, 2, 0, 4, 2), (0, 2, 0, 5, 2),
+    (1, 1, 1, 4, 2), (1, 1, 1, 5, 2), (1, 3, 0, 0, 0), (0, 2, 0, 6, 1), (0, 2, 1, 6, 1),
+    (0, 1, 0, 6, 1), (0, 1, 1, 6, 1), (1, 3, 1, 0, 0), (1, 2, 1, 0, 0), (1, 3, 0, 2, 0),
+    (1, 3, 1, 2, 0), (1, 2, 0, 1, 0), (3, ((0, (1,)), (1, (0,)), (2, (1,)), (3, (2,)))),
+    (1, 3, 0, 1, 0), (4, ((0, (1,)), (1, (0,)), (2, (1,)), (3, (2,)))), (1, 3, 1, 4, 2),
+    (1, 3, 1, 5, 2), (1, 0, 0, 2, 1), (1, 2, 0, 2, 0), (1, 2, 1, 2, 0), (1, 1, 1, 0, 2),
+    (3, ((0, (0,)), (2, (2,)))), (1, 3, 0, 3, 0), (1, 0, 1, 2, 1), (4, ((0, (0,)), (2, (2,)))),
+    (1, 0, 0, 0, 1), (1, 0, 1, 0, 1), (1, 0, 1, 1, 2), (1, 0, 1, 3, 2), (1, 2, 1, 3, 2),
+    (1, 3, 0, 6, 0), (1, 3, 1, 6, 0), (2, 1, 0, 0), (1, 1, 1, 2, 2), (1, 2, 1, 4, 2),
+    (1, 2, 1, 5, 2), (1, 1, 1, 1, 2), (1, 0, 0, 1, 1), (1, 2, 0, 6, 0), (1, 2, 1, 6, 0),
+    (1, 0, 0, 6, 1), (1, 0, 1, 6, 1), (1, 0, 0, 3, 1), (1, 3, 0, 4, 0), (1, 3, 0, 5, 0),
+    (1, 2, 0, 3, 0), (2, 1, 0, 2), (1, 2, 0, 4, 0), (1, 0, 0, 4, 1), (1, 0, 0, 5, 1),
+    (1, 1, 1, 6, 2), (2, 1, 0, 1), (1, 2, 0, 5, 0), (2, 1, 0, 3), (2, 1, 0, 6), (2, 1, 0, 4),
+    (2, 1, 0, 5),
 )
 
 PLAN = ((END_PROGRAM, MID_PROGRAM), PIECES)
@@ -157,9 +158,9 @@
 
 def plane_kernel(
     plan, tiles,
-    own, middle, weights, gate_in, up_in, down_in, sgate_in, sup_in, sdown_in,
+    own, middle, routes, route_weights, gate_in, up_in, down_in, sgate_in, sup_in, sdown_in,
     out,
-    rows_all, partial, from_level, from_side, table, scale,
+    weights, rows_all, partial, from_level, from_side, table, scale,
     gate, up, down, sgate, sup, sdown, hidden, shared,
     load_sem, twin_send, twin_recv, w_send, w_recv,
     row_recv, level_recv, side_recv, send_sem,
@@ -214,6 +215,13 @@
         pl.semaphore_signal(
             barrier, inc=1, device_id={"ep": lax.rem(me + step, experts)}, device_id_type=MESH
         )
+    expert = lax.broadcasted_iota(jnp.int32, (experts, rows), 0)
+    chosen = jnp.zeros((experts, rows), jnp.float32)
+    for k in range(routes.shape[0]):
+        chosen = chosen + jnp.where(expert == routes[k:k + 1, :], route_weights[k:k + 1, :], 0.0)
+    weights[...] = jnp.zeros_like(weights)
+    for n in range(nodes):
+        weights[n, 0:2, 0:rows] = chosen[2 * n:2 * n + 2]
     pl.semaphore_wait(barrier, experts - 1)
 
     def remote(src, dst, send, recv, target):
@@ -226,7 +234,7 @@
     for step in range(1, nodes):
         other = lax.rem(node + step, nodes)
         copy = remote(
-            weights.at[pl.ds(other * 2, 2)], table.at[node],
+            weights.at[other], table.at[node],
             w_send.at[step], w_recv.at[nodes - step], other * 2 + core,
         )
         copy.start()
@@ -271,7 +279,7 @@
             hidden[pl.ds(base, take), at] = factor(n, jax.nn.silu(g) * u).astype(jnp.bfloat16)
             return carry
 
-        lax.fori_loop(0, chunks, first, 0)
+        lax.fori_loop(0, chunks, first, 0, unroll=True)
 
     def feed_out(base, take, depth, down_w, finish):
         def second(n, carry):
@@ -283,7 +291,7 @@
             finish(cols, piece.astype(jnp.bfloat16))
             return carry
 
-        lax.fori_loop(0, width // 512, second, 0)
+        lax.fori_loop(0, width // 512, second, 0, unroll=True)
 
     halves = hid // 256
     depths = hidden.shape[0] // (4 * rows)
@@ -309,11 +317,11 @@
             remote(
                 table.at[other], table.at[other], w_send.at[step], w_recv.at[step], twin
             ).wait_recv()
-        table[node] = weights[pl.ds(node * 2, 2)]
+        table[node] = weights[node]
 
         def one(n, carry):
             for e in range(2):
-                line = jnp.broadcast_to(table[n, e], (128, 128))
+                line = jnp.broadcast_to(table[n, e:e + 1, :], (128, 128))
                 scale[e, pl.ds(pl.multiple_of(n * rows, tile), rows), :] = jnp.transpose(line)[:rows]
             return carry
 
@@ -524,9 +532,6 @@
     rows, width = second_normed.shape
     hid = expert_gate.shape[2]
     tiles = 6
-    chosen = routes[None, :, :] == jnp.arange(experts, dtype=jnp.int32)[:, None, None]
-    weights = jnp.sum(jnp.where(chosen, route_weights[None], 0.0), axis=2)
-    weights = jnp.pad(weights, ((0, 0), (0, 128 - rows)))[:, None, :]
     vmem = pl.BlockSpec(memory_space=pltpu.VMEM)
     hbm = pl.BlockSpec(memory_space=pl.ANY)
     dma = pltpu.SemaphoreType.DMA
@@ -537,14 +542,15 @@
     return pl.pallas_call(
         functools.partial(plane_kernel, PLAN, tiles),
         out_shape=jax.ShapeDtypeStruct((rows, width), half),
-        in_specs=[vmem] * 3 + [hbm] * 6,
+        in_specs=[vmem] * 4 + [hbm] * 6,
         out_specs=vmem,
         scratch_shapes=[
+            pltpu.VMEM((nodes, 8, 128), jnp.float32),
             pltpu.VMEM((nodes * rows, width), half),
             pltpu.VMEM((nodes * rows, width), half),
             pltpu.VMEM(((nodes + 2) * rows, width), half),
             pltpu.VMEM((nodes // 2 * rows, width), half),
-            pltpu.VMEM((nodes, 2, 1, 128), jnp.float32),
+            pltpu.VMEM((nodes, 8, 128), jnp.float32),
             pltpu.VMEM((2, nodes * rows, 128), jnp.float32),
             pltpu.VMEM((2, width, hid), half),
             pltpu.VMEM((2, width, hid), half),
@@ -565,86 +571,165 @@
             dma((most,)),
         ],
         compiler_params=pltpu.CompilerParams(
-            collective_id=0, has_side_effects=True, vmem_limit_bytes=60 * 1024 * 1024
+            collective_id=0, has_side_effects=True, vmem_limit_bytes=65011712
         ),
     )(
-        second_normed, middle, weights,
+        second_normed, middle, routes.T, route_weights.T,
         expert_gate, expert_up, expert_down, shared_gate, shared_up, shared_down,
     )
 
 
 def mixer_kernel(
-    tokens, prior, mix_gain, in_weight, params, input_map, output_map, skip, out_weight,
-    channel_gain, new_state, middle, second, normed, acts, acc,
+    tokens_in, prior_in, mix_gain_in, in_weight_in, decay_in, frequency_in, log_step_in,
+    input_map_in, output_map_in, skip_in, out_weight_in, channel_gain_in,
+    new_state, middle, second,
+    tokens, prior, mix_gain, in_weight, decay, frequency, log_step,
+    input_map, output_map, skip, out_weight, channel_gain,
+    params, table, normed, acts, first_sem, chunk_sem, tail_sem, out_sem,
 ):
-    step = pl.program_id(0)
     lane = 128
-    channels = in_weight.shape[1]
-    width = input_map.shape[2]
-    group = acts.shape[1] * width // prior.shape[2]
+    chunks, model, block = in_weight.shape
+    rows = tokens.shape[0]
+    groups, width = decay.shape
+    states = prior.shape[3]
+    group = chunks * block // groups
     per = lane // group
-    states = per * width
+    entries = per * width
+
+    firsts = [
+        pltpu.make_async_copy(src, dst, first_sem.at[n])
+        for n, (src, dst) in enumerate(
+            ((tokens_in, tokens), (mix_gain_in, mix_gain), (decay_in, decay),
+             (frequency_in, frequency), (log_step_in, log_step), (skip_in, skip),
+             (channel_gain_in, channel_gain))
+        )
+    ]
+
+    def chunk_copies(k):
+        cols = pl.ds(pl.multiple_of(k * block, block), block)
+        wide = pl.ds(pl.multiple_of(k * states, states), states)
+        return [
+            pltpu.make_async_copy(src, dst, chunk_sem.at[n, k])
+            for n, (src, dst) in enumerate(
+                ((in_weight_in.at[:, cols], in_weight.at[k]),
+                 (input_map_in.at[:, cols], input_map.at[k]),
+                 (output_map_in.at[:, cols], output_map.at[k]),
+                 (prior_in.at[:, :, wide], prior.at[k]))
+            )
+        ]
+
+    def leaving(k):
+        wide = pl.ds(pl.multiple_of(k * states, states), states)
+        return pltpu.make_async_copy(prior.at[k], new_state.at[:, :, wide], out_sem.at[k])
+
+    for copy in firsts:
+        copy.start()
+    for k in range(chunks):
+        for copy in chunk_copies(k):
+            copy.start()
+    tail = pltpu.make_async_copy(out_weight_in, out_weight, tail_sem.at[0])
+    tail.start()
 
     def scaled(values, gain):
         factor = lax.rsqrt(jnp.mean(values * values, axis=-1, keepdims=True) + norm_eps)
         return (values * factor * gain[...]).astype(jnp.bfloat16)
 
-    @pl.when(step == 0)
-    def _():
-        normed[...] = scaled(tokens[...].astype(jnp.float32), mix_gain)
-        acc[...] = jnp.zeros_like(acc)
-
-    drive = jnp.dot(normed[...], in_weight[...], preferred_element_type=jnp.float32)
-    drive = drive.astype(jnp.bfloat16)
-    row = lax.broadcasted_iota(jnp.int32, (lane, states), 0) // group
-    column = lax.broadcasted_iota(jnp.int32, (lane, states), 1) // width
+    for copy in firsts[2:]:
+        copy.wait()
+    diagonal = lax.broadcasted_iota(jnp.int32, (groups, groups), 0) == (
+        lax.broadcasted_iota(jnp.int32, (groups, groups), 1)
+    )
+    steps = jnp.where(diagonal, jnp.broadcast_to(log_step[...], (groups, groups)), 0.0)
+    step_size = jnp.exp(jnp.sum(steps, axis=1, keepdims=True))
+    real_rate = -decay[...]
+    angle = frequency[...] * step_size
+    magnitude = jnp.exp(real_rate * step_size)
+    turn_real = magnitude * jnp.cos(angle)
+    turn_imag = magnitude * jnp.sin(angle)
+    denominator = real_rate * real_rate + frequency[...] * frequency[...]
+    params[0] = turn_real
+    params[1] = turn_imag
+    params[2] = ((turn_real - 1.0) * real_rate + turn_imag * frequency[...]) / denominator
+    params[3] = (turn_imag * real_rate - (turn_real - 1.0) * frequency[...]) / denominator
+    for copy in firsts[:2]:
+        copy.wait()
+    normed[...] = scaled(tokens[...].astype(jnp.float32), mix_gain)
+    for n in range(4):
+        for g in range(0, groups, 2):
+            pair = jnp.concatenate([params[n, g:g + 1, :], params[n, g + 1:g + 2, :]], axis=1)
+            table[n:n + 1, g * width:(g + 2) * width] = pair
+
+    row = lax.broadcasted_iota(jnp.int32, (lane, entries), 0) // group
+    column = lax.broadcasted_iota(jnp.int32, (lane, entries), 1) // width
     own_group = row == column
 
-    def spread(table):
-        tiled = jnp.concatenate([table] * per, axis=1)
+    def spread(values):
+        tiled = jnp.concatenate([values] * per, axis=1)
         return jnp.where(own_group, tiled, 0.0).astype(jnp.bfloat16)
 
-    for sub in range(channels // lane):
-        cols = slice(sub * lane, (sub + 1) * lane)
-        ent = slice(sub * states, (sub + 1) * states)
-        part = drive[:, cols]
-        push_real = jnp.dot(
-            part, spread(input_map[0, cols, :]), preferred_element_type=jnp.float32
-        )
-        push_imag = jnp.dot(
-            part, spread(input_map[1, cols, :]), preferred_element_type=jnp.float32
-        )
-        turn_real, turn_imag = params[0:1, ent], params[1:2, ent]
-        hold_real, hold_imag = params[2:3, ent], params[3:4, ent]
-        old_real, old_imag = prior[0, :, ent], prior[1, :, ent]
-        fresh_real = (
-            turn_real * old_real - turn_imag * old_imag
-            + (push_real * hold_real - push_imag * hold_imag)
-        )
-        fresh_imag = (
-            turn_real * old_imag + turn_imag * old_real
-            + (push_real * hold_imag + push_imag * hold_real)
-        )
-        new_state[0, :, ent] = fresh_real
-        new_state[1, :, ent] = fresh_imag
-        across = (((1,), (1,)), ((), ()))
-        readout = lax.dot_general(
-            fresh_real.astype(jnp.bfloat16), spread(output_map[0, cols, :]), across,
-            preferred_element_type=jnp.float32,
-        ) - lax.dot_general(
-            fresh_imag.astype(jnp.bfloat16), spread(output_map[1, cols, :]), across,
-            preferred_element_type=jnp.float32,
-        )
-        readout = readout + skip[:, cols] * part.astype(jnp.float32)
-        acts[:, cols] = jax.nn.gelu(readout).astype(jnp.bfloat16)
-    acc[...] += jnp.dot(acts[...], out_weight[...], preferred_element_type=jnp.float32)
-
-    @pl.when(step == pl.num_programs(0) - 1)
-    def _():
-        mixed = acc[...].astype(jnp.bfloat16).astype(jnp.float32)
-        mid = (tokens[...].astype(jnp.float32) + mixed).astype(jnp.bfloat16)
-        middle[...] = mid
-        second[...] = scaled(mid.astype(jnp.float32), channel_gain)
+    across = (((1,), (1,)), ((), ()))
+
+    def chunk(k, carry):
+        for copy in chunk_copies(k):
+            copy.wait()
+        drive = jnp.dot(normed[...], in_weight[k], preferred_element_type=jnp.float32)
+        drive = drive.astype(jnp.bfloat16)
+        for sub in range(block // lane):
+            cols = slice(sub * lane, (sub + 1) * lane)
+            ent = slice(sub * entries, (sub + 1) * entries)
+            at = pl.ds(pl.multiple_of(k * states + sub * entries, entries), entries)
+            spot = pl.ds(pl.multiple_of(k * block + sub * lane, lane), lane)
+            part = drive[:, cols]
+            push_real = jnp.dot(
+                part, spread(input_map[k, 0, cols, :]), preferred_element_type=jnp.float32
+            )
+            push_imag = jnp.dot(
+                part, spread(input_map[k, 1, cols, :]), preferred_element_type=jnp.float32
+            )
+            turn_real, turn_imag = table[0:1, at], table[1:2, at]
+            hold_real, hold_imag = table[2:3, at], table[3:4, at]
+            old_real, old_imag = prior[k, 0, :, ent], prior[k, 1, :, ent]
+            fresh_real = (
+                turn_real * old_real - turn_imag * old_imag
+                + (push_real * hold_real - push_imag * hold_imag)
+            )
+            fresh_imag = (
+                turn_real * old_imag + turn_imag * old_real
+                + (push_real * hold_imag + push_imag * hold_real)
+            )
+            prior[k, 0, :, ent] = fresh_real
+            prior[k, 1, :, ent] = fresh_imag
+            readout = lax.dot_general(
+                fresh_real.astype(jnp.bfloat16), spread(output_map[k, 0, cols, :]), across,
+                preferred_element_type=jnp.float32,
+            ) - lax.dot_general(
+                fresh_imag.astype(jnp.bfloat16), spread(output_map[k, 1, cols, :]), across,
+                preferred_element_type=jnp.float32,
+            )
+            readout = readout + skip[:, spot] * part.astype(jnp.float32)
+            acts[:, spot] = jax.nn.gelu(readout).astype(jnp.bfloat16)
+        leaving(k).start()
+        return carry
+
+    lax.fori_loop(0, chunks, chunk, 0)
+    tail.wait()
+    wide = 512
+    total = jnp.zeros((rows, 1), jnp.float32)
+    for n in range(model // wide):
+        cols = slice(n * wide, (n + 1) * wide)
+        mixed = jnp.dot(acts[...], out_weight[:, cols], preferred_element_type=jnp.float32)
+        mixed = mixed.astype(jnp.bfloat16).astype(jnp.float32)
+        mid = (tokens[:, cols].astype(jnp.float32) + mixed).astype(jnp.bfloat16)
+        middle[:, cols] = mid
+        mid = mid.astype(jnp.float32)
+        total = total + jnp.sum(mid * mid, axis=-1, keepdims=True)
+    factor = lax.rsqrt(total / model + norm_eps)
+    for n in range(model // wide):
+        cols = slice(n * wide, (n + 1) * wide)
+        mid = middle[:, cols].astype(jnp.float32)
+        second[:, cols] = (mid * factor * channel_gain[:, cols]).astype(jnp.bfloat16)
+    for k in range(chunks):
+        leaving(k).wait()
 
 
 def mixer_stage(
@@ -654,60 +739,51 @@
     rows, model = tokens.shape
     groups, width = decay_rate.shape
     channels = in_weight.shape[1]
-    step_size = jnp.exp(log_step)[:, None]
-    real_rate = -decay_rate
-    magnitude = jnp.exp(real_rate * step_size)
-    turn_real = magnitude * jnp.cos(frequency * step_size)
-    turn_imag = magnitude * jnp.sin(frequency * step_size)
-    denominator = real_rate * real_rate + frequency * frequency
-    hold_real = ((turn_real - 1.0) * real_rate + turn_imag * frequency) / denominator
-    hold_imag = (turn_imag * real_rate - (turn_real - 1.0) * frequency) / denominator
-    params = jnp.stack([turn_real, turn_imag, hold_real, hold_imag]).reshape(4, -1)
     in_map = jnp.transpose(input_map, (0, 1, 3, 2)).reshape(2, channels, width)
     out_map = output_map.reshape(2, channels, width)
     block = 256
+    chunks = channels // block
     states = block * groups * width // channels
-
-    def whole(*shape):
-        return pl.BlockSpec(shape, lambda i: (0,) * len(shape))
-
     half = jnp.bfloat16
+    full = jnp.float32
+    hbm = pl.BlockSpec(memory_space=pl.ANY)
+    vmem = pl.BlockSpec(memory_space=pltpu.VMEM)
+    dma = pltpu.SemaphoreType.DMA
     return pl.pallas_call(
         mixer_kernel,
-        grid=(channels // block,),
         out_shape=(
-            jax.ShapeDtypeStruct(prior_state.shape, jnp.float32),
+            jax.ShapeDtypeStruct(prior_state.shape, full),
             jax.ShapeDtypeStruct((rows, model), half),
             jax.ShapeDtypeStruct((rows, model), half),
         ),
-        in_specs=[
-            whole(rows, model),
-            pl.BlockSpec((2, rows, states), lambda i: (0, 0, i)),
-            whole(1, model),
-            pl.BlockSpec((model, block), lambda i: (0, i)),
-            pl.BlockSpec((4, states), lambda i: (0, i)),
-            pl.BlockSpec((2, block, width), lambda i: (0, i, 0)),
-            pl.BlockSpec((2, block, width), lambda i: (0, i, 0)),
-            pl.BlockSpec((1, block), lambda i: (0, i)),
-            pl.BlockSpec((block, model), lambda i: (i, 0)),
-            whole(1, model),
-        ],
-        out_specs=(
-            pl.BlockSpec((2, rows, states), lambda i: (0, 0, i)),
-            whole(rows, model),
-            whole(rows, model),
-        ),
+        in_specs=[hbm] * 12,
+        out_specs=(hbm, vmem, vmem),
         scratch_shapes=[
             pltpu.VMEM((rows, model), half),
-            pltpu.VMEM((rows, block), half),
-            pltpu.VMEM((rows, model), jnp.float32),
+            pltpu.VMEM((chunks, 2, rows, states), full),
+            pltpu.VMEM((1, model), full),
+            pltpu.VMEM((chunks, model, block), half),
+            pltpu.VMEM((groups, width), full),
+            pltpu.VMEM((groups, width), full),
+            pltpu.VMEM((1, groups), full),
+            pltpu.VMEM((chunks, 2, block, width), full),
+            pltpu.VMEM((chunks, 2, block, width), full),
+            pltpu.VMEM((1, channels), full),
+            pltpu.VMEM((channels, model), half),
+            pltpu.VMEM((1, model), full),
+            pltpu.VMEM((4, groups, width), full),
+            pltpu.VMEM((4, groups * width), full),
+            pltpu.VMEM((rows, model), half),
+            pltpu.VMEM((rows, channels), half),
+            dma((7,)),
+            dma((4, chunks)),
+            dma((1,)),
+            dma((chunks,)),
         ],
-        compiler_params=pltpu.CompilerParams(
-            dimension_semantics=("arbitrary",), vmem_limit_bytes=62 * 1024 * 1024
-        ),
+        compiler_params=pltpu.CompilerParams(vmem_limit_bytes=65011712),
     )(
-        tokens, prior_state, mix_gain[None], in_weight, params, in_map, out_map,
-        skip_gain[None], out_weight, channel_gain[None],
+        tokens, prior_state, mix_gain[None], in_weight, decay_rate, frequency, log_step[None],
+        in_map, out_map, skip_gain[None], out_weight, channel_gain[None],
     )
 
 

time: 84.2 us -> 76.6 us (0.910)
  Pallas kernels: 77.5 us -> 74 us
  other arithmetic: 2.4 us -> 0 us
  local copies, waits for them, and re-layouts: 3.36 us -> 1.77 us
    pallas_call x1, Pallas kernels: 67.1 us -> 63.2 us  [plane_stage(): pl.pallas_call(functools.partial(plane_kernel, PLAN, tiles), out_shape=ja...]
    mul x1 -> x0, other arithmetic: 0.99 us -> none  [mixer_stage(): turn_real = magnitude * jnp.cos(frequency * step_size)]
where the time goes in v2:
time: 76.6 us; the launch traced here: 76.4 us
  Pallas kernels  74 us (97%)
  local copies, waits for them, and re-layouts  1.77 us (2%)
    pallas_call x1, Pallas kernels, plane_stage(): pl.pallas_call(functools.partial(plane_kernel, PLAN, tiles), out_shape=ja...  63.2 us
    pallas_call x1, Pallas kernels, mixer_stage(): pl.pallas_call(mixer_kernel, out_shape=(jax.ShapeDtypeStruct(prior_state....  10.8 us
    unnamed x1, local copies, waits for them, and re-layouts  1.77 us

profile of v2, /device:TPU:0, one launch (start us, length us, event | category | flops | bytes accessed | tf_op | source)
XLA Modules:
  0.0 76.4 jit_solution(6234624637648948352)
XLA Ops:
  0.6 10.8 %shard_map.203 = (f32[2,96,4096]{2,1,0:T(8,128)}, bf16[96,2048]{1,0:T(8,128)(2,1)}, bf16[96,2048]{1,0:T(8,128)(2,1)}) custom-call(bf16[96,2048]{1,0:T(8,128)(2,1)} %tokens_in.1, f32[2,96,4096]{2,1,0:T(8,128)} %prior_in.1, f32[1,2048]{1,0:T(1,128)} %bitcast.12, bf16[2048,1024]{1,0:T(8,128)(2,1)} %in_weight_in.1, f32[64,64]{1,0:T(8,128)} %decay_in.1, ...), custom_call_target="tpu_custom_call" | custom-call | tf_op jit(solution)/shard_map/pallas_call | solution.py:752
  11.4 63.2 %shard_map.204 = bf16[96,2048]{1,0:T(8,128)(2,1)} custom-call(bf16[96,2048]{1,0:T(8,128)(2,1)} %get-tuple-element.5.own, bf16[96,2048]{1,0:T(8,128)(2,1)} %get-tuple-element.6.middle, s32[6,96]{1,0:T(8,128)} %bitcast.14, f32[6,96]{1,0:T(8,128)} %bitcast.15, bf16[1,2048,512]{2,1,0:T(8,128)(2,1)} %gate_in.1, bf16[1,2048,512]{2,1,0:T(8,128)(2,1)} %up_in.1, ...), custom_call_target="tpu_custom_call" | custom-call | tf_op jit(solution)/shard_map/pallas_call | solution.py:542
  74.6 1.8 %copy.23 = bf16[96,2048]{1,0:T(8,128)(2,1)} copy(bf16[96,2048]{1,0:T(8,128)(2,1)} %shard_map.204) | data formatting | bytes 786432

commit v3 on v2

--- a/solution.py
+++ b/solution.py
@@ -100,25 +100,25 @@
     (0, 0, 0, 0, 2), (0, 0, 0, 0, 0), (0, 0, 0, 1, 2), (0, 0, 0, 1, 0), (0, 0, 0, 3, 2),
     (0, 0, 0, 2, 2), (0, 0, 0, 3, 0), (5,), (0, 0, 1, 0, 0), (0, 0, 0, 2, 0), (0, 0, 0, 4, 0),
     (0, 1, 0, 1, 2), (0, 1, 0, 3, 2), (0, 0, 0, 4, 2), (0, 0, 1, 2, 0), (0, 0, 0, 5, 0),
-    (0, 0, 0, 6, 0), (0, 2, 0, 1, 2), (0, 0, 0, 5, 2), (0, 0, 0, 6, 2),
-    (3, ((0, (1,)), (1, (0,)))), (4, ((0, (1,)), (1, (0,)))), (1, 1, 0, 0, 0), (1, 1, 1, 0, 0),
-    (1, 1, 1, 1, 2), (0, 3, 0, 1, 2), (1, 0, 1, 3, 2), (0, 0, 1, 6, 0), (3, ((2, (0,)),)),
-    (4, ((2, (0,)),)), (1, 2, 0, 0, 0), (1, 2, 1, 0, 0), (1, 2, 1, 1, 2), (1, 1, 0, 1, 0),
-    (0, 3, 0, 3, 2), (3, ((3, (0,)),)), (0, 2, 0, 3, 2), (4, ((3, (0,)),)), (1, 3, 0, 0, 0),
-    (1, 3, 1, 0, 0), (1, 3, 1, 1, 2), (1, 2, 0, 1, 0), (3, ((0, (0,)), (3, (1,)))),
-    (4, ((0, (0,)), (3, (1,)))), (1, 3, 0, 2, 0), (1, 3, 1, 2, 0), (1, 3, 1, 3, 2),
-    (1, 0, 1, 1, 2), (3, ((2, (1,)),)), (1, 3, 0, 1, 0), (4, ((2, (1,)),)), (1, 2, 0, 2, 0),
-    (1, 2, 1, 2, 0), (1, 2, 1, 3, 2), (0, 3, 0, 4, 2), (0, 3, 0, 5, 2), (1, 3, 0, 3, 0),
-    (3, ((1, (1,)),)), (0, 2, 0, 4, 2), (4, ((1, (1,)),)), (1, 2, 0, 3, 0), (1, 1, 0, 2, 0),
-    (1, 1, 1, 3, 2), (0, 2, 0, 5, 2), (3, ((3, (2,)),)), (0, 1, 0, 4, 2), (4, ((3, (2,)),)),
-    (1, 3, 0, 6, 0), (1, 3, 1, 4, 2), (1, 3, 1, 5, 2), (0, 1, 0, 5, 2), (1, 3, 1, 6, 0),
-    (1, 1, 1, 2, 0), (3, ((2, (2,)),)), (4, ((2, (2,)),)), (1, 2, 0, 6, 0), (1, 2, 1, 4, 2),
-    (1, 2, 1, 5, 2), (1, 2, 1, 6, 0), (1, 3, 0, 4, 0), (1, 0, 1, 2, 2), (1, 3, 0, 5, 0),
-    (1, 1, 0, 3, 0), (3, ((0, (2,)), (1, (2,)))), (4, ((0, (2,)), (1, (2,)))), (1, 2, 0, 4, 0),
-    (1, 1, 0, 6, 0), (1, 1, 1, 4, 2), (1, 1, 1, 6, 0), (1, 0, 1, 0, 2), (1, 1, 1, 5, 2),
-    (1, 0, 1, 4, 2), (1, 2, 0, 5, 0), (2, 0, 0, 2), (2, 0, 0, 1), (2, 0, 0, 0), (1, 0, 1, 6, 2),
-    (1, 0, 1, 5, 2), (1, 1, 0, 4, 0), (1, 1, 0, 5, 0), (2, 0, 0, 3), (2, 0, 0, 6), (2, 0, 0, 4),
-    (2, 0, 0, 5),
+    (0, 0, 0, 6, 0), (0, 2, 0, 1, 2), (0, 0, 0, 5, 2), (0, 0, 0, 6, 2), (3, ((1, (0,)),)),
+    (4, ((1, (0,)),)), (1, 1, 0, 0, 0), (1, 1, 1, 0, 0), (1, 1, 1, 1, 2), (0, 3, 0, 1, 2),
+    (0, 0, 1, 6, 0), (3, ((2, (0,)),)), (4, ((2, (0,)),)), (1, 2, 0, 0, 0), (1, 2, 1, 0, 0),
+    (1, 2, 1, 1, 2), (1, 1, 0, 1, 0), (0, 3, 0, 3, 2), (3, ((0, (1,)), (3, (0,)))),
+    (0, 2, 0, 3, 2), (4, ((0, (1,)), (3, (0,)))), (1, 3, 0, 0, 0), (1, 3, 1, 0, 0),
+    (1, 3, 1, 1, 2), (1, 0, 1, 3, 2), (1, 2, 0, 1, 0), (3, ((3, (1,)),)), (4, ((3, (1,)),)),
+    (1, 3, 0, 2, 0), (1, 3, 1, 2, 0), (1, 3, 1, 3, 2), (3, ((0, (2,)), (2, (1,)))),
+    (0, 3, 0, 4, 2), (1, 3, 0, 1, 0), (4, ((0, (2,)), (2, (1,)))), (1, 2, 1, 3, 2),
+    (0, 3, 0, 5, 2), (1, 0, 1, 4, 2), (1, 3, 0, 3, 0), (1, 2, 0, 2, 0), (1, 2, 1, 2, 0),
+    (3, ((1, (1,)),)), (0, 2, 0, 4, 2), (4, ((1, (1,)),)), (1, 2, 0, 3, 0), (1, 1, 1, 3, 2),
+    (0, 2, 0, 5, 2), (1, 0, 1, 5, 2), (3, ((3, (2,)),)), (4, ((3, (2,)),)), (1, 3, 0, 6, 0),
+    (1, 3, 1, 4, 2), (1, 3, 1, 5, 2), (0, 1, 0, 4, 2), (0, 1, 0, 5, 2), (1, 3, 1, 6, 0),
+    (1, 1, 0, 2, 0), (1, 1, 1, 2, 0), (3, ((0, (0,)), (2, (2,)))), (4, ((0, (0,)), (2, (2,)))),
+    (1, 2, 1, 4, 2), (1, 2, 1, 5, 2), (1, 3, 0, 4, 0), (1, 3, 0, 5, 0), (1, 2, 0, 6, 0),
+    (1, 2, 1, 6, 0), (1, 1, 0, 3, 0), (1, 0, 1, 2, 2), (1, 0, 1, 1, 2), (3, ((1, (2,)),)),
+    (1, 2, 0, 4, 0), (2, 0, 0, 3), (4, ((1, (2,)),)), (1, 2, 0, 5, 0), (1, 1, 0, 6, 0),
+    (1, 1, 1, 4, 2), (1, 1, 1, 5, 2), (1, 1, 1, 6, 0), (2, 0, 0, 2), (1, 0, 1, 0, 2),
+    (1, 0, 1, 6, 2), (1, 1, 0, 4, 0), (1, 1, 0, 5, 0), (2, 0, 0, 1), (2, 0, 0, 0), (2, 0, 0, 6),
+    (2, 0, 0, 4), (2, 0, 0, 5),
 )
 
 MID_PROGRAM = (
@@ -131,26 +131,26 @@
     (0, 1, 1, 2, 0), (0, 0, 0, 4, 0), (0, 3, 1, 0, 1), (0, 0, 0, 5, 0), (0, 1, 0, 4, 0),
     (0, 1, 0, 5, 0), (0, 3, 0, 3, 2), (0, 0, 0, 5, 2), (0, 1, 0, 4, 2), (0, 1, 0, 5, 2),
     (0, 1, 0, 6, 2), (0, 3, 0, 3, 1), (0, 2, 0, 3, 1), (0, 0, 0, 6, 0), (0, 3, 0, 2, 1),
-    (0, 3, 1, 2, 1), (0, 2, 0, 2, 1), (0, 0, 1, 6, 0), (0, 1, 0, 6, 0),
-    (3, ((0, (2,)), (3, (1,)))), (0, 2, 1, 2, 1), (4, ((0, (2,)), (3, (1,)))), (0, 3, 0, 4, 2),
-    (0, 3, 0, 4, 1), (1, 3, 1, 3, 2), (1, 0, 1, 4, 2), (1, 0, 1, 5, 2), (0, 1, 1, 6, 0),
-    (0, 3, 0, 5, 1), (0, 1, 0, 2, 1), (0, 1, 1, 2, 1), (3, ((1, (1, 2)), (2, (0,)), (3, (0,)))),
-    (0, 2, 0, 4, 1), (0, 2, 0, 5, 1), (4, ((1, (1, 2)), (2, (0,)), (3, (0,)))), (0, 3, 0, 6, 1),
-    (0, 3, 1, 6, 1), (0, 1, 0, 4, 1), (0, 1, 0, 5, 1), (1, 3, 1, 1, 2), (1, 2, 0, 0, 0),
-    (1, 2, 1, 1, 2), (0, 3, 0, 5, 2), (1, 1, 1, 3, 2), (0, 2, 0, 4, 2), (0, 2, 0, 5, 2),
-    (1, 1, 1, 4, 2), (1, 1, 1, 5, 2), (1, 3, 0, 0, 0), (0, 2, 0, 6, 1), (0, 2, 1, 6, 1),
-    (0, 1, 0, 6, 1), (0, 1, 1, 6, 1), (1, 3, 1, 0, 0), (1, 2, 1, 0, 0), (1, 3, 0, 2, 0),
-    (1, 3, 1, 2, 0), (1, 2, 0, 1, 0), (3, ((0, (1,)), (1, (0,)), (2, (1,)), (3, (2,)))),
-    (1, 3, 0, 1, 0), (4, ((0, (1,)), (1, (0,)), (2, (1,)), (3, (2,)))), (1, 3, 1, 4, 2),
-    (1, 3, 1, 5, 2), (1, 0, 0, 2, 1), (1, 2, 0, 2, 0), (1, 2, 1, 2, 0), (1, 1, 1, 0, 2),
-    (3, ((0, (0,)), (2, (2,)))), (1, 3, 0, 3, 0), (1, 0, 1, 2, 1), (4, ((0, (0,)), (2, (2,)))),
-    (1, 0, 0, 0, 1), (1, 0, 1, 0, 1), (1, 0, 1, 1, 2), (1, 0, 1, 3, 2), (1, 2, 1, 3, 2),
-    (1, 3, 0, 6, 0), (1, 3, 1, 6, 0), (2, 1, 0, 0), (1, 1, 1, 2, 2), (1, 2, 1, 4, 2),
-    (1, 2, 1, 5, 2), (1, 1, 1, 1, 2), (1, 0, 0, 1, 1), (1, 2, 0, 6, 0), (1, 2, 1, 6, 0),
-    (1, 0, 0, 6, 1), (1, 0, 1, 6, 1), (1, 0, 0, 3, 1), (1, 3, 0, 4, 0), (1, 3, 0, 5, 0),
-    (1, 2, 0, 3, 0), (2, 1, 0, 2), (1, 2, 0, 4, 0), (1, 0, 0, 4, 1), (1, 0, 0, 5, 1),
-    (1, 1, 1, 6, 2), (2, 1, 0, 1), (1, 2, 0, 5, 0), (2, 1, 0, 3), (2, 1, 0, 6), (2, 1, 0, 4),
-    (2, 1, 0, 5),
+    (0, 3, 1, 2, 1), (0, 2, 0, 2, 1), (3, ((2, (0,)), (3, (0, 1)))), (0, 2, 1, 2, 1),
+    (0, 0, 1, 6, 0), (0, 1, 0, 6, 0), (4, ((2, (0,)), (3, (0, 1)))), (0, 3, 0, 4, 2),
+    (0, 3, 0, 4, 1), (1, 3, 1, 1, 2), (1, 3, 1, 3, 2), (1, 2, 1, 1, 2),
+    (3, ((0, (1, 2)), (1, (1,)), (2, (1,)))), (0, 1, 1, 6, 0), (0, 3, 0, 5, 1), (0, 1, 0, 2, 1),
+    (0, 1, 1, 2, 1), (0, 2, 0, 4, 1), (0, 2, 0, 5, 1), (1, 2, 0, 0, 0), (1, 2, 1, 0, 0),
+    (4, ((0, (1, 2)), (1, (1,)), (2, (1,)))), (0, 3, 0, 6, 1), (0, 3, 1, 6, 1), (0, 1, 0, 4, 1),
+    (0, 1, 0, 5, 1), (1, 2, 1, 3, 2), (1, 0, 1, 3, 2), (1, 0, 1, 4, 2), (1, 0, 1, 5, 2),
+    (1, 1, 1, 3, 2), (0, 3, 0, 5, 2), (0, 2, 0, 4, 2), (0, 2, 0, 5, 2), (1, 3, 0, 0, 0),
+    (0, 2, 0, 6, 1), (0, 2, 1, 6, 1), (0, 1, 0, 6, 1), (1, 3, 1, 0, 0), (1, 2, 0, 1, 0),
+    (1, 3, 0, 2, 0), (1, 3, 1, 2, 0), (1, 3, 0, 1, 0), (1, 3, 0, 3, 0), (1, 0, 0, 2, 1),
+    (0, 1, 1, 6, 1), (1, 2, 0, 2, 0), (3, ((1, (0, 2)), (3, (2,)))), (1, 0, 1, 2, 1),
+    (1, 2, 1, 2, 0), (4, ((1, (0, 2)), (3, (2,)))), (1, 3, 1, 4, 2), (1, 3, 1, 5, 2),
+    (1, 3, 0, 6, 0), (1, 2, 0, 3, 0), (1, 1, 1, 0, 2), (1, 0, 0, 3, 1),
+    (3, ((0, (0,)), (2, (2,)))), (1, 3, 1, 6, 0), (4, ((0, (0,)), (2, (2,)))), (1, 0, 0, 0, 1),
+    (1, 0, 1, 0, 1), (1, 0, 1, 1, 2), (1, 2, 1, 4, 2), (1, 2, 1, 5, 2), (1, 1, 1, 2, 2),
+    (1, 1, 1, 1, 2), (1, 1, 1, 4, 2), (1, 1, 1, 5, 2), (1, 0, 0, 6, 1), (1, 3, 0, 4, 0),
+    (1, 3, 0, 5, 0), (1, 0, 1, 6, 1), (2, 1, 0, 0), (1, 2, 0, 6, 0), (1, 2, 1, 6, 0),
+    (1, 0, 0, 1, 1), (2, 1, 0, 3), (1, 0, 0, 4, 1), (1, 0, 0, 5, 1), (1, 2, 0, 4, 0),
+    (1, 2, 0, 5, 0), (2, 1, 0, 2), (1, 1, 1, 6, 2), (2, 1, 0, 1), (2, 1, 0, 4), (2, 1, 0, 5),
+    (2, 1, 0, 6),
 )
 
 PLAN = ((END_PROGRAM, MID_PROGRAM), PIECES)
@@ -158,12 +158,12 @@
 
 def plane_kernel(
     plan, tiles,
-    own, middle, routes, route_weights, gate_in, up_in, down_in, sgate_in, sup_in, sdown_in,
+    own_in, middle_in, routes_in, route_weights_in, gate_in, up_in, down_in, sgate_in, sup_in, sdown_in,
     out,
-    weights, rows_all, partial, from_level, from_side, table, scale,
+    middle, routes, route_weights, weights, rows_all, partial, from_level, from_side, table, scale,
     gate, up, down, sgate, sup, sdown, hidden, shared,
     load_sem, twin_send, twin_recv, w_send, w_recv,
-    row_recv, level_recv, side_recv, send_sem,
+    row_recv, level_recv, side_recv, send_sem, entry_sem,
 ):
     programs, pieces = plan
     experts = lax.axis_size("ep")
@@ -174,7 +174,7 @@
     level = node // 2
     nodes = experts // 2
     top = nodes // 2 - 1
-    rows, width = own.shape
+    rows, width = own_in.shape
     tile = rows // tiles
     hid = sgate.shape[1]
     flipped = level * 2 > top
@@ -207,21 +207,23 @@
             )
         )
     ]
-    for load in loads:
-        load.start()
+    home = pl.ds(pl.multiple_of(node * rows, tile), rows)
+    entry = [
+        pltpu.make_async_copy(src, dst, entry_sem.at[n])
+        for n, (src, dst) in enumerate(
+            ((own_in, rows_all.at[home]), (routes_in, routes),
+             (route_weights_in, route_weights), (middle_in, middle))
+        )
+    ]
+    for copy in entry + loads:
+        copy.start()
 
     barrier = pltpu.get_barrier_semaphore()
     for step in range(1, experts):
         pl.semaphore_signal(
             barrier, inc=1, device_id={"ep": lax.rem(me + step, experts)}, device_id_type=MESH
         )
-    expert = lax.broadcasted_iota(jnp.int32, (experts, rows), 0)
-    chosen = jnp.zeros((experts, rows), jnp.float32)
-    for k in range(routes.shape[0]):
-        chosen = chosen + jnp.where(expert == routes[k:k + 1, :], route_weights[k:k + 1, :], 0.0)
-    weights[...] = jnp.zeros_like(weights)
-    for n in range(nodes):
-        weights[n, 0:2, 0:rows] = chosen[2 * n:2 * n + 2]
+    entry[0].wait()
     pl.semaphore_wait(barrier, experts - 1)
 
     def remote(src, dst, send, recv, target):
@@ -230,15 +232,28 @@
             device_id={"ep": target}, device_id_type=MESH,
         )
 
-    always = []
-    for step in range(1, nodes):
-        other = lax.rem(node + step, nodes)
-        copy = remote(
-            weights.at[other], table.at[node],
-            w_send.at[step], w_recv.at[nodes - step], other * 2 + core,
-        )
-        copy.start()
-        always.append(copy)
+    table_sends = [
+        remote(
+            weights.at[lax.rem(node + step, nodes)], table.at[node],
+            w_send.at[step], w_recv.at[nodes - step],
+            lax.rem(node + step, nodes) * 2 + core,
+        )
+        for step in range(1, nodes)
+    ]
+
+    def send_table():
+        for copy in entry[1:]:
+            copy.wait()
+        expert = lax.broadcasted_iota(jnp.int32, (experts, rows), 0)
+        chosen = jnp.zeros((experts, rows), jnp.float32)
+        for k in range(routes.shape[0]):
+            chosen = chosen + jnp.where(expert == routes[k:k + 1, :], route_weights[k:k + 1, :], 0.0)
+        weights[...] = jnp.zeros_like(weights)
+        for n in range(nodes):
+            weights[n, 0:2, 0:rows] = chosen[2 * n:2 * n + 2]
+        for copy in table_sends:
+            copy.start()
+
     twins = [
         remote(src, dst, twin_send.at[n], twin_recv.at[n], twin)
         for n, (src, dst) in enumerate(
@@ -304,7 +319,7 @@
             cols = pl.ds(pl.multiple_of(n * 256, 256), 256)
             return sgate[:, cols], sup[:, cols]
 
-        feed_in(0, lambda: own[...], rows, gates, halves, lambda n, value: value)
+        feed_in(0, lambda: rows_all[home, :], rows, gates, halves, lambda n, value: value)
 
         def keep(cols, piece):
             shared[:, cols] = piece
@@ -354,12 +369,9 @@
         def pass_row(q, rel, piece, way):
             row_in(q, rel, piece)
             origin = to_node(q, rel)
-            if (q, rel) == (position, 0):
-                src = own.at[region(0, piece)]
-            else:
-                src = rows_all.at[region(origin, piece)]
             push(
-                src, rows_all.at[region(origin, piece)], row_recv.at[origin, piece],
+                rows_all.at[region(origin, piece)], rows_all.at[region(origin, piece)],
+                row_recv.at[origin, piece],
                 neighbour(way) * 2 + core,
             )
 
@@ -510,7 +522,7 @@
             elif kind == 5:
                 for copy in twins:
                     copy.start()
-                rows_all[pl.ds(pl.multiple_of(node * rows, tile), rows), :] = own[...]
+                send_table()
                 shared_expert()
         for copy in sends:
             copy.wait_send()
@@ -519,7 +531,7 @@
     for position, program in enumerate(programs):
         near_end = jnp.logical_or(level == position, level == top - position)
         pl.when(near_end)(functools.partial(run, program, position))
-    for copy in always + twins:
+    for copy in table_sends + twins:
         copy.wait_send()
 
 
@@ -542,9 +554,12 @@
     return pl.pallas_call(
         functools.partial(plane_kernel, PLAN, tiles),
         out_shape=jax.ShapeDtypeStruct((rows, width), half),
-        in_specs=[vmem] * 4 + [hbm] * 6,
+        in_specs=[hbm] * 10,
         out_specs=vmem,
         scratch_shapes=[
+            pltpu.VMEM((rows, width), half),
+            pltpu.VMEM((routes.shape[1], rows), jnp.int32),
+            pltpu.VMEM((routes.shape[1], rows), jnp.float32),
             pltpu.VMEM((nodes, 8, 128), jnp.float32),
             pltpu.VMEM((nodes * rows, width), half),
             pltpu.VMEM((nodes * rows, width), half),
@@ -569,9 +584,10 @@
             dma((nodes + 2, count)),
             dma((nodes // 2, count)),
             dma((most,)),
+            dma((4,)),
         ],
         compiler_params=pltpu.CompilerParams(
-            collective_id=0, has_side_effects=True, vmem_limit_bytes=65011712
+            collective_id=0, has_side_effects=True, vmem_limit_bytes=62 * 1024 * 1024
         ),
     )(
         second_normed, middle, routes.T, route_weights.T,
@@ -608,27 +624,43 @@
     def chunk_copies(k):
         cols = pl.ds(pl.multiple_of(k * block, block), block)
         wide = pl.ds(pl.multiple_of(k * states, states), states)
+        views = [
+            (input_map_in.at[:, cols], input_map.at[k]),
+            (output_map_in.at[:, cols], output_map.at[k]),
+        ]
+        for n in range(4):
+            part = pl.ds(n * model // 4, model // 4)
+            views.append((in_weight_in.at[part, cols], in_weight.at[k, part]))
+        for n in range(2):
+            views.append((prior_in.at[n, :, wide], prior.at[k, n]))
         return [
             pltpu.make_async_copy(src, dst, chunk_sem.at[n, k])
-            for n, (src, dst) in enumerate(
-                ((in_weight_in.at[:, cols], in_weight.at[k]),
-                 (input_map_in.at[:, cols], input_map.at[k]),
-                 (output_map_in.at[:, cols], output_map.at[k]),
-                 (prior_in.at[:, :, wide], prior.at[k]))
-            )
+            for n, (src, dst) in enumerate(views)
         ]
 
     def leaving(k):
         wide = pl.ds(pl.multiple_of(k * states, states), states)
         return pltpu.make_async_copy(prior.at[k], new_state.at[:, :, wide], out_sem.at[k])
 
+    def begin(k):
+        for copy in chunk_copies(k):
+            copy.start()
+
+    tails = []
+    for n in range(8):
+        part = pl.ds(n * chunks * block // 8, chunks * block // 8)
+        tails.append(
+            pltpu.make_async_copy(out_weight_in.at[part], out_weight.at[part], tail_sem.at[n])
+        )
+
+    def begin_tail():
+        for copy in tails:
+            copy.start()
+
     for copy in firsts:
         copy.start()
-    for k in range(chunks):
-        for copy in chunk_copies(k):
-            copy.start()
-    tail = pltpu.make_async_copy(out_weight_in, out_weight, tail_sem.at[0])
-    tail.start()
+    begin(0)
+    begin(1)
 
     def scaled(values, gain):
         factor = lax.rsqrt(jnp.mean(values * values, axis=-1, keepdims=True) + norm_eps)
@@ -653,6 +685,7 @@
     params[3] = (turn_imag * real_rate - (turn_real - 1.0) * frequency[...]) / denominator
     for copy in firsts[:2]:
         copy.wait()
+    begin(2)
     normed[...] = scaled(tokens[...].astype(jnp.float32), mix_gain)
     for n in range(4):
         for g in range(0, groups, 2):
@@ -672,6 +705,8 @@
     def chunk(k, carry):
         for copy in chunk_copies(k):
             copy.wait()
+        pl.when(k + 3 < chunks)(lambda: begin(k + 3))
+        pl.when(k + 3 == chunks)(begin_tail)
         drive = jnp.dot(normed[...], in_weight[k], preferred_element_type=jnp.float32)
         drive = drive.astype(jnp.bfloat16)
         for sub in range(block // lane):
@@ -712,7 +747,8 @@
         return carry
 
     lax.fori_loop(0, chunks, chunk, 0)
-    tail.wait()
+    for copy in tails:
+        copy.wait()
     wide = 512
     total = jnp.zeros((rows, 1), jnp.float32)
     for n in range(model // wide):
@@ -776,11 +812,11 @@
             pltpu.VMEM((rows, model), half),
             pltpu.VMEM((rows, channels), half),
             dma((7,)),
-            dma((4, chunks)),
-            dma((1,)),
+            dma((8, chunks)),
+            dma((8,)),
             dma((chunks,)),
         ],
-        compiler_params=pltpu.CompilerParams(vmem_limit_bytes=65011712),
+        compiler_params=pltpu.CompilerParams(vmem_limit_bytes=62 * 1024 * 1024),
     )(
         tokens, prior_state, mix_gain[None], in_weight, decay_rate, frequency, log_step[None],
         in_map, out_map, skip_gain[None], out_weight, channel_gain[None],

time: 76.6 us -> 73.9 us (0.965)
  Pallas kernels: 74 us -> 71.3 us
    pallas_call x1, Pallas kernels: 63.2 us -> 61.8 us  [plane_stage(): pl.pallas_call(functools.partial(plane_kernel, PLAN, tiles), out_shape=ja...]
    pallas_call x1, Pallas kernels: 10.8 us -> 9.52 us  [mixer_stage(): pl.pallas_call(mixer_kernel, out_shape=(jax.ShapeDtypeStruct(prior_state....]
where the time goes in v3:
time: 73.9 us; the launch traced here: 73.7 us
  Pallas kernels  71.3 us (96%)
  local copies, waits for them, and re-layouts  1.77 us (2%)
    pallas_call x1, Pallas kernels, plane_stage(): pl.pallas_call(functools.partial(plane_kernel, PLAN, tiles), out_shape=ja...  61.8 us
    pallas_call x1, Pallas kernels, mixer_stage(): pl.pallas_call(mixer_kernel, out_shape=(jax.ShapeDtypeStruct(prior_state....  9.52 us
    unnamed x1, local copies, waits for them, and re-layouts  1.77 us

profile of v3, /device:TPU:0, one launch (start us, length us, event | category | flops | bytes accessed | tf_op | source)
XLA Modules:
  0.0 73.7 jit_solution(10622007766301494975)
XLA Ops:
  0.6 9.5 %shard_map.203 = (f32[2,96,4096]{2,1,0:T(8,128)}, bf16[96,2048]{1,0:T(8,128)(2,1)}, bf16[96,2048]{1,0:T(8,128)(2,1)}) custom-call(bf16[96,2048]{1,0:T(8,128)(2,1)} %tokens_in.1, f32[2,96,4096]{2,1,0:T(8,128)} %prior_in.1, f32[1,2048]{1,0:T(1,128)} %bitcast.12, bf16[2048,1024]{1,0:T(8,128)(2,1)} %in_weight_in.1, f32[64,64]{1,0:T(8,128)} %decay_in.1, ...), custom_call_target="tpu_custom_call" | custom-call | tf_op jit(solution)/shard_map/pallas_call | solution.py:788
  10.2 61.8 %shard_map.204 = bf16[96,2048]{1,0:T(8,128)(2,1)} custom-call(bf16[96,2048]{1,0:T(8,128)(2,1)} %get-tuple-element.5.own_in, bf16[96,2048]{1,0:T(8,128)(2,1)} %get-tuple-element.6.middle_in, s32[6,96]{1,0:T(8,128)} %bitcast.14, f32[6,96]{1,0:T(8,128)} %bitcast.15, bf16[1,2048,512]{2,1,0:T(8,128)(2,1)} %gate_in.1, bf16[1,2048,512]{2,1,0:T(8,128)(2,1)} %up_in.1, ...), custom_call_target="tpu_custom_call" | custom-call | tf_op jit(solution)/shard_map/pallas_call | solution.py:554
  71.9 1.8 %copy.23 = bf16[96,2048]{1,0:T(8,128)(2,1)} copy(bf16[96,2048]{1,0:T(8,128)(2,1)} %shard_map.204) | data formatting | bytes 786432
